TPU v7x, 512 devices: a whole 4x8x8 slice. The times are simulated.
512 devices in a mesh: sp: 64 (over z, y), tp: 8 (over x, core).
Axes of the slice: x: 4, y: 8, z: 8, core: 2. Of those that a mesh axis runs over, the one named last changes fastest.
Arguments:
- latent: bfloat16 [16384, 2048], P(('sp', 'tp')), may hold values from -6 to 6
- context: bfloat16 [512, 2048], P('sp'), may hold values from -6 to 6
- condition: float32 [2048], P('tp'), may hold values from -6 to 6
- context_condition: float32 [2048], P('tp'), may hold values from -6 to 6
- modulation_weight: bfloat16 [2048, 6144], P('tp', 'sp'), may hold values from -0.125 to 0.125
- query_first: bfloat16 [2048, 512], P(None, 'tp'), may hold values from -1 to 1
- query_second: bfloat16 [2048, 512], P(None, 'tp'), may hold values from -1 to 1
- key_first: bfloat16 [2048, 512], P(None, 'tp'), may hold values from -1 to 1
- key_second: bfloat16 [2048, 512], P(None, 'tp'), may hold values from -1 to 1
- value_weight: bfloat16 [2048, 1024], P(None, 'tp'), may hold values from -0.125 to 0.125
- lambda_head: float32 [8], P('tp'), may hold values from 0.3 to 0.8
- context_score_boost: float32 [8], P('tp'), may hold values from 1.5 to 3
- head_gain: float32 [128], replicated, may hold values from 0.1 to 1.9
- output_weight: bfloat16 [1024, 2048], P('tp'), may hold values from -0.1875 to 0.1875
Outputs:
- updated: bfloat16 [16384, 2048], P(('sp', 'tp'))
All inputs are finite; a program needn't handle non-finite values.
Results may differ from a plain program's by a relative error of at most 0.0095.
Values may be sent and summed in bfloat16 or wider, within the bound.
A program may use at most 64 MiB of HBM per device.

v0:
```python
import jax
import jax.numpy as jnp
from jax import lax
from jax.sharding import PartitionSpec as P

HEAD_DIM = 64
VALUE_DIM = 128
GRID_W = 64


EPSILON = 1e-06
THETA = 10000.0
NEGATIVE = -1e30


def copy_for_each(shard, axis):
    size = lax.axis_size(axis)
    return lax.all_to_all(
        jnp.broadcast_to(shard[None], (size, *shard.shape)), axis, 0, 0, tiled=True
    )


def taken_together(shard, axis):
    return copy_for_each(shard, axis).sum(axis=0)


def joined_along(tiles, dim):
    tiles = jnp.moveaxis(tiles, 0, dim)
    lengths = tiles.shape
    return tiles.reshape(*lengths[:dim], lengths[dim] * lengths[dim + 1], *lengths[dim + 2 :])


def collect(shard, axis, dim):
    return joined_along(copy_for_each(shard, axis), dim)


def in_one_piece(arrays, axis, dim, along):
    widths = [a.shape[along] for a in arrays]
    both = jnp.concatenate(arrays, axis=along)
    out = lax.all_gather(both, axis, axis=dim, tiled=True)
    return tuple(jnp.split(out, [sum(widths[:k]) for k in range(1, len(widths))], axis=along))


def in_blocks(shard, dim, size):
    before, after = (shard.shape[:dim], shard.shape[dim + 1 :])
    return jnp.moveaxis(shard.reshape(*before, size, -1, *after), dim, 0)


def sum_at_owner(shard, axis, dim):
    tiles = in_blocks(shard, dim, lax.axis_size(axis))
    arrived = lax.all_to_all(tiles, axis, split_axis=0, concat_axis=0, tiled=True)
    return arrived.astype(jnp.float32).sum(axis=0)


def norm_rows(rows):
    values = rows.astype(jnp.float32)
    return values * lax.rsqrt(jnp.mean(values * values, axis=-1, keepdims=True) + EPSILON)


def rotate_pairs(values, positions):
    half = values.shape[-1] // 2
    quarter = half // 2
    reciprocal_norm = THETA ** (-jnp.arange(quarter, dtype=jnp.float32) / quarter)

    def turn(part, where):
        angle = where.astype(jnp.float32)[:, None] * reciprocal_norm[None, :]
        cosine_table = jnp.concatenate([jnp.cos(angle)] * 2, -1)[:, None, :]
        sine = jnp.concatenate([jnp.sin(angle)] * 2, -1)[:, None, :]
        flipped = jnp.concatenate([-part[..., quarter:], part[..., :quarter]], -1)
        return part * cosine_table + flipped * sine

    grid_row = positions // GRID_W
    grid_col = positions % GRID_W
    return jnp.concatenate(
        [turn(values[..., :half], grid_row), turn(values[..., half:], grid_col)], -1
    )


def block_extent(rows):
    size = min(rows, 1024)
    while rows % size:
        size -= 1
    return size


def body(
    latent,
    context,
    condition,
    context_condition,
    modulation_weight,
    query_first,
    query_second,
    key_first,
    key_second,
    value_weight,
    lambda_head,
    context_score_boost,
    head_gain,
    output_weight,
):
    width = latent.shape[1]
    signal = jax.nn.silu(jnp.stack([condition, context_condition])).astype(jnp.bfloat16)
    partial_mod = jnp.dot(signal, modulation_weight, preferred_element_type=jnp.float32)
    reduced = taken_together(partial_mod, "tp")
    modulation = collect(reduced, "sp", 1)
    shift = modulation[:, :width]
    scale = modulation[:, width : 2 * width]
    gate = modulation[:, 2 * width :]
    h_latent = (norm_rows(latent) * (1.0 + scale[0]) + shift[0]).astype(jnp.bfloat16)
    h_context = (norm_rows(context) * (1.0 + scale[1]) + shift[1]).astype(jnp.bfloat16)
    heads_dev = value_weight.shape[1] // VALUE_DIM
    span = heads_dev * HEAD_DIM
    offset = lax.axis_index("sp") * (latent.shape[0] * lax.axis_size("tp"))
    piece = collect(h_latent, "tp", 0)
    count = piece.shape[0]
    positions = offset + jnp.arange(count, dtype=jnp.int32)
    turned = []
    for weight in (query_first, query_second, key_first, key_second):
        product = jnp.dot(piece, weight, preferred_element_type=jnp.float32).reshape(
            count, heads_dev, HEAD_DIM
        )
        turned.append(rotate_pairs(product, positions).astype(jnp.bfloat16).reshape(count, span))
    values = jnp.dot(piece, value_weight, preferred_element_type=jnp.float32).astype(jnp.bfloat16)
    projected = jnp.concatenate(turned + [values], axis=1)
    queries = projected.shape[0]
    queries_one = projected[:, :span].reshape(queries, heads_dev, HEAD_DIM)
    queries_two = projected[:, span : 2 * span].reshape(queries, heads_dev, HEAD_DIM)
    latent_keys = projected[:, 2 * span : 4 * span]
    latent_values = projected[:, 4 * span :]

    def update(carry, block):
        keys_pair, values, boolean_markers = block
        count = keys_pair.shape[0]
        keys_one = keys_pair[:, :span].reshape(count, heads_dev, HEAD_DIM)
        keys_two = keys_pair[:, span:].reshape(count, heads_dev, HEAD_DIM)
        values_heads = values.reshape(count, heads_dev, VALUE_DIM)
        extra_score = context_score_boost[:, None, None] * boolean_markers[None, None, :]
        renewed = []
        for (highest, totals, weighted), query, keys in zip(
            carry, (queries_one, queries_two), (keys_one, keys_two)
        ):
            scores = (
                jnp.einsum("qhd,khd->hqk", query, keys, preferred_element_type=jnp.float32)
                * HEAD_DIM ** (-0.5)
                + extra_score
            )
            peak = jnp.maximum(highest, jnp.max(scores, axis=-1))
            exp_weights = jnp.exp(scores - peak[..., None])
            rescale = jnp.exp(highest - peak)
            totals = totals * rescale + jnp.sum(exp_weights, axis=-1)
            weighted = weighted * jnp.transpose(rescale)[:, :, None] + jnp.einsum(
                "hqk,khe->qhe",
                exp_weights.astype(jnp.bfloat16),
                values_heads,
                preferred_element_type=jnp.float32,
            )
            renewed.append((peak, totals, weighted))
        return (tuple(renewed), None)

    def fold_keys(carry, keys_pair, values, boolean_markers):
        rows = keys_pair.shape[0]
        size = block_extent(rows)
        count = rows // size
        blocks = (
            keys_pair.reshape(count, size, keys_pair.shape[1]),
            values.reshape(count, size, values.shape[1]),
            boolean_markers.reshape(count, size),
        )
        carry, unused = lax.scan(update, carry, blocks)
        return carry

    start_state = (
        jnp.full((heads_dev, queries), NEGATIVE, jnp.float32),
        jnp.zeros((heads_dev, queries), jnp.float32),
        jnp.zeros((queries, heads_dev, VALUE_DIM), jnp.float32),
    )
    initial = (start_state, start_state)
    keys_pair = jnp.concatenate(
        [
            jnp.dot(h_context, key_first, preferred_element_type=jnp.float32).astype(jnp.bfloat16),
            jnp.dot(h_context, key_second, preferred_element_type=jnp.float32).astype(jnp.bfloat16),
        ],
        axis=1,
    )
    values = jnp.dot(h_context, value_weight, preferred_element_type=jnp.float32).astype(
        jnp.bfloat16
    )
    all_keys, all_values = in_one_piece((keys_pair, values), "sp", 0, 1)
    carry = fold_keys(initial, all_keys, all_values, jnp.ones((all_keys.shape[0],), jnp.float32))
    pieces = (
        lax.all_gather(latent_keys, "sp", axis=0, tiled=True),
        lax.all_gather(latent_values, "sp", axis=0, tiled=True),
    )
    boolean_markers = jnp.zeros((pieces[0].shape[0],), jnp.float32)
    final = fold_keys(carry, pieces[0], pieces[1], boolean_markers)
    outcomes = [weighted / jnp.transpose(totals)[:, :, None] for highest, totals, weighted in final]
    mixed = outcomes[0] - lambda_head[None, :, None] * outcomes[1]
    normed = (
        mixed * lax.rsqrt(jnp.mean(mixed * mixed, axis=-1, keepdims=True) + EPSILON) * head_gain
    )
    heads_out = normed.astype(jnp.bfloat16).reshape(queries, heads_dev * VALUE_DIM)
    branch = sum_at_owner(
        jnp.dot(heads_out, output_weight, preferred_element_type=jnp.float32).astype(jnp.bfloat16),
        "tp",
        0,
    )
    return (latent.astype(jnp.float32) + gate[0] * branch).astype(jnp.bfloat16)


def solution(mesh):
    in_specs = (
        P(("sp", "tp"), None),
        P("sp", None),
        P("tp"),
        P("tp"),
        P("tp", "sp"),
        P(None, "tp"),
        P(None, "tp"),
        P(None, "tp"),
        P(None, "tp"),
        P(None, "tp"),
        P("tp"),
        P("tp"),
        P(),
        P("tp", None),
    )
    out_specs = P(("sp", "tp"), None)
    return jax.shard_map(body, mesh=mesh, in_specs=in_specs, out_specs=out_specs, check_vma=False)
```

profile of v0, /device:TPU:1, one launch (start us, length us, event | category | flops | bytes accessed | tf_op | source)
XLA Modules:
  0.0 344.7 jit_solution(9492942217073333725)
XLA Ops:
  8.2 10.1 %all-to-all-start = ((f32[8,2,96]{2,1,0:T(2,128)}), f32[8,2,96]{2,1,0:T(2,128)S(1)}, u32[]{:S(2)}, u32[]{:S(2)}) async-start(f32[8,2,96]{2,1,0:T(2,128)} %broadcast_in_dim.22), calls=%async_computation | async-start | bytes 16384 | tf_op jit(solution)/shard_map/all_to_all | solution.py:18
  19.3 3.6 %all-to-all-done = f32[8,2,96]{2,1,0:T(2,128)S(1)} async-done(((f32[8,2,96]{2,1,0:T(2,128)}), f32[8,2,96]{2,1,0:T(2,128)S(1)}, u32[]{:S(2)}, u32[]{:S(2)}) %all-to-all-start) | async-done | bytes 6176 | tf_op jit(solution)/shard_map/all_to_all | solution.py:18
  23.6 12.0 %all-to-all-start.1 = ((f32[64,2,96]{2,1,0:T(2,128)}), f32[64,2,96]{2,1,0:T(2,128)S(1)}, u32[]{:S(2)}, u32[]{:S(2)}) async-start(f32[64,2,96]{2,1,0:T(2,128)} %broadcast_in_dim.23), calls=%async_computation.1 | async-start | bytes 131072 | tf_op jit(solution)/shard_map/all_to_all | solution.py:18
  35.6 11.1 %all-to-all-done.1 = f32[64,2,96]{2,1,0:T(2,128)S(1)} async-done(((f32[64,2,96]{2,1,0:T(2,128)}), f32[64,2,96]{2,1,0:T(2,128)S(1)}, u32[]{:S(2)}, u32[]{:S(2)}) %all-to-all-start.1) | async-done | bytes 49184 | tf_op jit(solution)/shard_map/all_to_all | solution.py:18
  49.0 5.7 %all-to-all-start.2 = ((bf16[8,32,2048]{2,1,0:T(8,128)(2,1)}), bf16[8,32,2048]{2,1,0:T(8,128)(2,1)S(1)}, u32[]{:S(2)}, u32[]{:S(2)}) async-start(bf16[8,32,2048]{2,1,0:T(8,128)(2,1)} %broadcast_in_dim.25), calls=%async_computation.2 | async-start | bytes 2097152 | tf_op jit(solution)/shard_map/all_to_all | solution.py:18
  55.0 14.8 %all-to-all-done.2 = bf16[8,32,2048]{2,1,0:T(8,128)(2,1)S(1)} async-done(((bf16[8,32,2048]{2,1,0:T(8,128)(2,1)}), bf16[8,32,2048]{2,1,0:T(8,128)(2,1)S(1)}, u32[]{:S(2)}, u32[]{:S(2)}) %all-to-all-start.2) | async-done | bytes 1048608 | tf_op jit(solution)/shard_map/all_to_all | solution.py:18
  74.8 35.7 %all_gather.9 = bf16[512,256]{1,0:T(8,128)(2,1)S(1)} all-gather(bf16[8,256]{1,0:T(8,128)(2,1)S(1)} %pad_maximum_fusion.5), channel_id=1, replica_groups=mesh['sp'=64,'tp'=8] {'sp'}, dimensions={0}, use_global_device_ids=true | all-gather | bytes 266240 | tf_op jit(solution)/shard_map/all_gather | solution.py:40
  113.4 35.7 %all-gather.3.cloned.1.call-done = bf16[16384,128]{0,1:T(8,128)(2,1)} async-done(((bf16[256,128]{0,1:T(8,128)(2,1)}), bf16[16384,128]{0,1:T(8,128)(2,1)}) %all-gather.3.cloned.1.call-update) | async-done | bytes 4194320 | tf_op jit(solution)/shard_map/all_gather | solution.py:192
  149.0 6.4 %copy.26 = bf16[16384,128]{1,0:T(8,128)(2,1)} copy(bf16[16384,128]{0,1:T(8,128)(2,1)} %all-gather.3.cloned.1.call-done) | data formatting | bytes 8388608 | tf_op jit(solution)/shard_map/while | solution.py:170
  155.4 79.0 %all-gather.5.cloned.1.call-done = bf16[16384,128]{1,0:T(8,128)(2,1)} async-done(((bf16[256,128]{1,0:T(8,128)(2,1)}), bf16[16384,128]{1,0:T(8,128)(2,1)}) %all-gather.5.cloned.1.call-update) | async-done | bytes 4194320 | tf_op jit(solution)/shard_map/all_gather | solution.py:193
  234.5 78.2 %while.4 = (s32[]{:T(128)}, f32[1,256]{1,0:T(1,128)S(1)}, f32[1,256]{1,0:T(1,128)S(1)}, f32[256,1,128]{0,2,1:T(8,128)S(1)}, f32[1,256]{1,0:T(1,128)S(1)}, /*inde...) while((s32[]{:T(128)}, f32[1,256]{1,0:T(1,128)S(1)}, ...), condition=%wide.region_12.13_spmd, body=%wide.region_7.12_spmd.sunk | while | flops 205128704 | bytes 8488073 | solution.py:170
  238.0 1.3 fusion.139
  242.9 1.3 fusion.139
  247.8 1.3 fusion.139
  252.6 1.3 fusion.139
  257.5 1.3 fusion.139
  262.4 1.3 fusion.139
  267.3 1.3 fusion.139
  272.2 1.3 fusion.139
  277.1 1.3 fusion.139
  281.9 1.3 fusion.139
  286.8 1.3 fusion.139
  291.7 1.3 fusion.139
  313.2 23.8 %all_to_all.20 = bf16[8,32,2048]{2,1,0:T(8,128)(2,1)S(1)} all-to-all(bf16[8,32,2048]{2,1,0:T(8,128)(2,1)S(1)} %bitcast.183), channel_id=1, replica_groups=mesh['sp'=64,'tp'=8] {'tp'}, dimensions={0} | all-to-all | bytes 2097152 | tf_op jit(solution)/shard_map/all_to_all | solution.py:51
  (253 shorter events, 74.9 us)
Async XLA Ops:
  6.5 306.2 %copy-start = (bf16[128,2048]{1,0:T(8,128)(2,1)S(1)}, bf16[128,2048]{1,0:T(8,128)(2,1)}, u32[]{:S(2)}) copy-start(bf16[128,2048]{1,0:T(8,128)(2,1)} %param.29) | copy-start | bytes 1572868
  6.5 63.2 %copy-start.3 = (bf16[2048,64]{0,1:T(8,128)(2,1)S(1)}, bf16[2048,64]{0,1:T(8,128)(2,1)}, u32[]{:S(2)}) copy-start(bf16[2048,64]{0,1:T(8,128)(2,1)} %param.23) | copy-start | bytes 786436
  6.5 63.7 %copy-start.4 = (bf16[2048,64]{0,1:T(8,128)(2,1)S(1)}, bf16[2048,64]{0,1:T(8,128)(2,1)}, u32[]{:S(2)}) copy-start(bf16[2048,64]{0,1:T(8,128)(2,1)} %param.24) | copy-start | bytes 786436
  6.5 64.9 %copy-start.1 = (bf16[2048,128]{1,0:T(8,128)(2,1)S(1)}, bf16[2048,128]{1,0:T(8,128)(2,1)}, u32[]{:S(2)}) copy-start(bf16[2048,128]{1,0:T(8,128)(2,1)} %param.25) | copy-start | bytes 1572868
  8.2 14.7 %all-to-all-start = ((f32[8,2,96]{2,1,0:T(2,128)}), f32[8,2,96]{2,1,0:T(2,128)S(1)}, u32[]{:S(2)}, u32[]{:S(2)}) async-start(f32[8,2,96]{2,1,0:T(2,128)} %broadcast_in_dim.22), calls=%async_computation | async-start | bytes 16384 | tf_op jit(solution)/shard_map/all_to_all | solution.py:18
  23.6 23.1 %all-to-all-start.1 = ((f32[64,2,96]{2,1,0:T(2,128)}), f32[64,2,96]{2,1,0:T(2,128)S(1)}, u32[]{:S(2)}, u32[]{:S(2)}) async-start(f32[64,2,96]{2,1,0:T(2,128)} %broadcast_in_dim.23), calls=%async_computation.1 | async-start | bytes 131072 | tf_op jit(solution)/shard_map/all_to_all | solution.py:18
  47.9 25.9 %copy-start.7 = (bf16[8,2048]{1,0:T(8,128)(2,1)S(1)}, bf16[8,2048]{1,0:T(8,128)(2,1)}, u32[]{:S(2)}) copy-start(bf16[8,2048]{1,0:T(8,128)(2,1)} %param.17) | copy-start | bytes 98308
  49.0 61.5 %copy-start.5 = (bf16[2048,64]{0,1:T(8,128)(2,1)S(1)}, bf16[2048,64]{0,1:T(8,128)(2,1)}, u32[]{:S(2)}) copy-start(bf16[2048,64]{0,1:T(8,128)(2,1)} %param.22) | copy-start | bytes 786436
  49.0 20.7 %all-to-all-start.2 = ((bf16[8,32,2048]{2,1,0:T(8,128)(2,1)}), bf16[8,32,2048]{2,1,0:T(8,128)(2,1)S(1)}, u32[]{:S(2)}, u32[]{:S(2)}) async-start(bf16[8,32,2048]{2,1,0:T(8,128)(2,1)} %broadcast_in_dim.25), calls=%async_computation.2 | async-start | bytes 2097152 | tf_op jit(solution)/shard_map/all_to_all | solution.py:18
  54.7 94.3 %all-gather.3.cloned.1.call-start = ((), (), s32[]{:S(2)}) async-start(), calls=%async_computation.4 | async-start | bytes 4259840 | tf_op jit(solution)/shard_map/all_gather | solution.py:192
  69.7 41.2 %copy-start.6 = (bf16[2048,64]{0,1:T(8,128)(2,1)S(1)}, bf16[2048,64]{0,1:T(8,128)(2,1)}, u32[]{:S(2)}) copy-start(bf16[2048,64]{0,1:T(8,128)(2,1)} %param.21) | copy-start | bytes 786436
  71.4 163.1 %all-gather.5.cloned.1.call-start = ((), (), s32[]{:S(2)}) async-start(), calls=%async_computation.5 | async-start | bytes 4259840 | tf_op jit(solution)/shard_map/all_gather | solution.py:193
  234.5 78.2 %copy-start.8 = (f32[128]{0:T(128)S(1)}, f32[128]{0:T(128)}, u32[]{:S(2)}) copy-start(f32[128]{0:T(128)} %param.28) | copy-start | bytes 1540
  312.6 24.6 %copy-start.2 = (bf16[32,2048]{1,0:T(8,128)(2,1)S(1)}, bf16[32,2048]{1,0:T(8,128)(2,1)}, u32[]{:S(2)}) copy-start(bf16[32,2048]{1,0:T(8,128)(2,1)} %param.16) | copy-start | bytes 393220
Sparse Core Ops, SparseCore 0:
  71.5 77.4 all-gather.2
  152.1 82.3 all-gather.4
where the time goes:
time: 347 us; the launch traced here: 345 us
  waiting for transfers between devices  144 us (41%)
  matrix products  60.3 us (17%)
  blocking collectives  59.5 us (17%)
  starting transfers between devices  27.8 us (8%)
  local copies, waits for them, and re-layouts  24.6 us (7%)
  between operations  14.9 us (4%)
  other arithmetic  12.3 us (4%)
    all_gather x1, waiting for transfers between devices, body(): lax.all_gather(latent_values, 'sp', axis=0, tiled=True)  79 us
    dot_general x34, matrix products, update(): jnp.einsum('hqk,khe->qhe', exp_weights.astype(jnp.bfloat16), values_heads...  43.2 us
    all_gather x1, blocking collectives, in_one_piece(): out = lax.all_gather(both, axis, axis=dim, tiled=True)  35.7 us
    all_gather x1, waiting for transfers between devices, body(): lax.all_gather(latent_keys, 'sp', axis=0, tiled=True)  35.7 us
    all_to_all x3, waiting for transfers between devices, copy_for_each(): lax.all_to_all(jnp.broadcast_to(shard[None], (size, *shard.shape)), axis,...  29.4 us
    all_to_all x3, starting transfers between devices, copy_for_each(): lax.all_to_all(jnp.broadcast_to(shard[None], (size, *shard.shape)), axis,...  27.8 us
    all_to_all x1, blocking collectives, sum_at_owner(): lax.all_to_all(tiles, axis, split_axis=0, concat_axis=0, tiled=True)  23.8 us
    squeeze x16, local copies, waits for them, and re-layouts, fold_keys(): carry, unused = lax.scan(update, carry, blocks)  15.6 us
  transfers between devices with their start and end apart: 5, of which 5 were waited for; matrix products, arithmetic and copies ran while one was open for 4% of the time, Pallas kernels for 0%

commit v1 on v0

v1 whole, which is shorter than its diff:
```python
import functools
import math

import jax
import jax.numpy as jnp
import numpy as np
from jax import lax
from jax.experimental import pallas as pl
from jax.experimental.pallas import tpu as pltpu
from jax.sharding import PartitionSpec as P

MESH = pl.DeviceIdType.MESH
EPSILON = 1e-06
THETA = 10000.0
GRID_W = 64
RING = 8
TP = 8
ROWS = 32
BLOCK = 256
CTX = 8
KEYS = BLOCK + 2 * CTX
WIDTH = 2048
CHUNK = 96
LOG2E = math.log2(math.e)
BF16 = jnp.bfloat16
F32 = jnp.float32

NT = (((1,), (1,)), ((), ()))
NN = (((1,), (0,)), ((), ()))


def dot(a, b, dims=NN):
    return lax.dot_general(a, b, dims, preferred_element_type=F32)


def remote(src, dst, send, recv, sp, tp):
    return pltpu.make_async_remote_copy(
        src_ref=src, dst_ref=dst, send_sem=send, recv_sem=recv, device_id=(sp, tp), device_id_type=MESH
    )


def silu(v):
    return v / (1.0 + jnp.exp(-v))


def kernel(
    latent, context, cond, ccond, modw, wq1, wq2, wk1, wk2, wv, lam, boost, gain, wout, freq,
    out,
    lat, ctx, mw, w64, wcat, wo, part, modg, modv, h, cosb, sinb, qb, kvb, vx, kc,
    osend, ssend, orecv, srecv, hsend, hrecv,
    load, part_s, part_r, y_s, y_r, z_s, z_r, lat_s, lat_r, latf_s, wo_s, wo_r, wof_s,
    q_s, q_r, kv_s, kv_r, o_s, o_r, st_s, st_r, h_s, h_r,
):
    sp, tp = lax.axis_index("sp"), lax.axis_index("tp")
    z, y = sp // RING, sp % RING
    x, core = tp // 2, tp % 2
    partner = x * 2 + 1 - core
    a = core * z + (1 - core) * y
    b = core * y + (1 - core) * z

    def at_a(i):
        return (1 - core) * (z * RING + i) + core * (i * RING + y)

    def at_b(i):
        return (1 - core) * (i * RING + y) + core * (z * RING + i)

    def chip(d):
        return ((x + d) % 4) * 2 + core

    loads = [
        pltpu.make_async_copy(modw, mw, load.at[0]),
        pltpu.make_async_copy(latent, lat.at[tp], load.at[1]),
        pltpu.make_async_copy(context, ctx, load.at[2]),
        pltpu.make_async_copy(wout, wo.at[tp], load.at[3]),
        pltpu.make_async_copy(wq1, w64.at[0], load.at[4]),
        pltpu.make_async_copy(wq2, w64.at[1], load.at[5]),
        pltpu.make_async_copy(wk1, w64.at[2], load.at[6]),
        pltpu.make_async_copy(wk2, w64.at[3], load.at[7]),
        pltpu.make_async_copy(wv, wcat.at[:, 256:384], load.at[8]),
    ]
    for c in loads:
        c.start()

    barrier = pltpu.get_barrier_semaphore()
    for d in range(1, TP):
        pl.semaphore_signal(barrier, inc=1, device_id=(sp, (tp + d) % TP), device_id_type=MESH)
    for d in range(1, RING):
        pl.semaphore_signal(barrier, inc=1, device_id=(at_a((a + d) % RING), tp), device_id_type=MESH)
        pl.semaphore_signal(barrier, inc=1, device_id=(at_b((b + d) % RING), tp), device_id_type=MESH)

    loads[0].wait()
    signal = silu(jnp.concatenate([cond[...], ccond[...], jnp.zeros((6, 256), F32)], axis=0)).astype(BF16)
    mine = dot(signal, mw[...])[0:2]
    part[0] = jnp.concatenate([mine, jnp.zeros((2, 128 - CHUNK), F32)], axis=1)
    loads[1].wait()
    loads[3].wait()
    pl.semaphore_wait(barrier, TP - 1 + 2 * (RING - 1))

    parts = [
        remote(part.at[0], part.at[d], part_s.at[d], part_r.at[d], sp, (tp + d) % TP) for d in range(1, TP)
    ]
    for c in parts:
        c.start()
    lats = [remote(lat.at[tp], lat.at[tp], lat_s.at[d], lat_r.at[tp], sp, chip(d)) for d in range(1, 4)]
    lats.append(remote(lat.at[tp], lat.at[tp], lat_s.at[0], lat_r.at[tp], sp, partner))
    for c in lats:
        c.start()
    wos = [remote(wo.at[tp], wo.at[tp], wo_s.at[d], wo_r.at[tp], sp, chip(d)) for d in range(1, 4)]
    wos.append(remote(wo.at[tp], wo.at[tp], wo_s.at[0], wo_r.at[tp], sp, partner))
    for c in wos:
        c.start()

    for c in parts:
        c.wait_recv()
    total = part[0]
    for d in range(1, TP):
        total = total + part[d]
    modg[z, y] = total
    ys = [
        remote(modg.at[z, y], modg.at[z, y], y_s.at[d], y_r.at[y], z * RING + (y + d) % RING, tp)
        for d in range(1, RING)
    ]
    for c in ys:
        c.start()

    row = lax.broadcasted_iota(jnp.int32, (BLOCK, 128), 0)
    lane = lax.broadcasted_iota(jnp.int32, (BLOCK, 128), 1)
    token = row + sp * BLOCK
    grid_row = token // GRID_W
    where = jnp.where(lane % 64 < 32, grid_row, token - grid_row * GRID_W).astype(F32)
    angle = where * freq[...]
    cosb[...] = jnp.cos(angle)
    sinb[...] = jnp.where(lane % 32 < 16, -jnp.sin(angle), jnp.sin(angle))

    for d in range(1, RING):
        other = (y + d) % RING
        remote(modg.at[z, other], modg.at[z, other], y_s.at[0], y_r.at[other], sp, tp).wait_recv()
    zs = [
        remote(modg.at[z], modg.at[z], z_s.at[d], z_r.at[z], ((z + d) % RING) * RING + y, tp)
        for d in range(1, RING)
    ]
    for c in zs:
        c.start()

    for c in loads[4:]:
        c.wait()
    wcat[:, 0:128] = jnp.concatenate([w64[0], w64[1]], axis=1)
    wcat[:, 128:256] = jnp.concatenate([w64[2], w64[3]], axis=1)
    ones = jnp.ones((BLOCK, 128), BF16)
    for j in range(RING):
        vx[j, :, 128:256] = ones
    vx[RING, :, 128:256] = ones
    fwd = []
    for d in range(1, 4):
        slot = chip(d)
        remote(lat.at[slot], lat.at[slot], lat_s.at[d], lat_r.at[slot], sp, tp).wait_recv()
        c = remote(lat.at[slot], lat.at[slot], latf_s.at[d], lat_r.at[slot], sp, partner)
        c.start()
        fwd.append(c)

    for d in range(1, RING):
        other = (z + d) % RING
        remote(modg.at[other], modg.at[other], z_s.at[0], z_r.at[other], sp, tp).wait_recv()

    lane2 = lax.broadcasted_iota(jnp.int32, (2, 128), 1)
    for g in range(16):
        c0, c1, c2, c3 = [modg[g // 2, (g % 2) * 4 + j] for j in range(4)]
        c1, c2, c3 = pltpu.roll(c1, 96, 1), pltpu.roll(c2, 64, 1), pltpu.roll(c3, 32, 1)
        rows = [jnp.where(lane2 < 96, c0, c1), jnp.where(lane2 < 64, c1, c2), jnp.where(lane2 < 32, c2, c3)]
        for m in range(3):
            for r in range(2):
                modv[r, 3 * g + m : 3 * g + m + 1, :] = rows[m][r : r + 1]

    loads[2].wait()

    def modulated(v, r):
        scaled = v * lax.rsqrt(jnp.mean(v * v, axis=1, keepdims=True) + EPSILON)
        pieces = []
        for k in range(WIDTH // 128):
            piece = scaled[:, k * 128 : (k + 1) * 128]
            piece = piece * (1.0 + modv[r, 16 + k : 17 + k, :]) + modv[r, k : k + 1, :]
            pieces.append(piece)
        return jnp.concatenate(pieces, axis=1)

    hc = modulated(ctx[...].astype(F32), 1)
    h[BLOCK:KEYS, :] = jnp.concatenate([hc, jnp.zeros((CTX, WIDTH), F32)], axis=0).astype(BF16)

    for d in range(4):
        slot = ((x + d) % 4) * 2 + 1 - core
        remote(lat.at[slot], lat.at[slot], lat_s.at[0], lat_r.at[slot], sp, tp).wait_recv()

    def fill(i, carry):
        v = lat[i // 2, pl.ds(pl.multiple_of((i % 2) * 16, 16), 16), :].astype(F32)
        h[pl.ds(pl.multiple_of(i * 16, 16), 16), :] = modulated(v, 0).astype(BF16)
        return carry

    lax.fori_loop(0, BLOCK // 16, fill, 0)

    qkv = dot(h[...], wcat[...])
    cosine, sine = cosb[...], sinb[...]

    def rope(v):
        turned = jnp.where(lane % 32 < 16, pltpu.roll(v, 112, 1), pltpu.roll(v, 16, 1))
        return v * cosine + turned * sine

    qb[0] = (rope(qkv[0:BLOCK, 0:128]) * (LOG2E / 8.0)).astype(BF16)
    kvb[0, 0:BLOCK, 0:128] = rope(qkv[0:BLOCK, 128:256]).astype(BF16)
    kvb[0, BLOCK:KEYS, 0:128] = qkv[BLOCK:KEYS, 128:256].astype(BF16)
    kvb[0, :, 128:256] = qkv[:, 256:384].astype(BF16)

    kvs = [
        remote(kvb.at[0], kvb.at[d], kv_s.at[d], kv_r.at[d], at_b((b + d) % RING), tp) for d in range(1, RING)
    ]
    qs = [remote(qb.at[0], qb.at[d], q_s.at[d], q_r.at[d], at_a((a + d) % RING), tp) for d in range(1, RING)]
    for i in (0, 6, 1, 5, 2, 4, 3):
        qs[i].start()
        kvs[i].start()
    for i in (0, 6, 1, 5, 2, 4, 3):
        qs[i].wait_recv()
        kvs[i].wait_recv()

    for j in range(RING):
        vx[j, :, 0:128] = kvb[j, 0:BLOCK, 128:256]
        kc[j * 16 : (j + 1) * 16, :] = kvb[j, BLOCK:KEYS, 0:128]
        vx[RING, j * 16 : (j + 1) * 16, 0:128] = kvb[j, BLOCK:KEYS, 128:256]
    lane1 = lax.broadcasted_iota(jnp.int32, (1, 128), 1)
    bias = jnp.where(lane1 % 16 < CTX, boost[0] * LOG2E, -1e30)
    laneq = lax.broadcasted_iota(jnp.int32, (BLOCK, 128), 1)

    def attend(query):
        scores = [dot(query, kvb[j, 0:BLOCK, 0:128], NT) for j in range(RING)]
        extra = dot(query, kc[...], NT) + bias
        peak = scores[0]
        for s in scores[1:]:
            peak = jnp.maximum(peak, s)
        peak = jnp.maximum(jnp.maximum(peak[:, 0:128], peak[:, 128:256]), extra)
        peak = jnp.max(peak, axis=1, keepdims=True)
        acc = dot(jnp.exp2(extra - peak).astype(BF16), vx[RING, 0:128, :])
        for j in range(RING):
            acc = acc + dot(jnp.exp2(scores[j] - peak).astype(BF16), vx[j])
        sums = acc[:, 128:256]
        return (acc[:, 0:128] / sums).astype(BF16), peak + jnp.log2(sums)

    def block(k):
        d = (4 + ((k + 1) // 2) * (1 - 2 * (k % 2))) % RING
        query = qb[d]
        none = jnp.zeros_like(query)
        one, level_one = attend(jnp.where(laneq < 64, query, none))
        two, level_two = attend(jnp.where(laneq < 64, none, query))
        osend[k, :, 0:128] = one
        osend[k, :, 128:256] = two
        levels = jnp.where(laneq % 8 < 4, level_one, level_two)
        ssend[k] = jnp.transpose(levels)[0:8, :]
        return d

    def back(k, carry):
        d = block(k)
        to = at_a((a - d + RING) % RING)
        remote(ssend.at[k], srecv.at[d], st_s.at[k], st_r.at[d], to, tp).start()
        remote(osend.at[k], orecv.at[d], o_s.at[k], o_r.at[d], to, tp).start()
        return carry

    lax.fori_loop(0, 4, back, 0)
    wofwd = []
    for d in range(1, 4):
        slot = chip(d)
        remote(wo.at[slot], wo.at[slot], wo_s.at[d], wo_r.at[slot], sp, tp).wait_recv()
        c = remote(wo.at[slot], wo.at[slot], wof_s.at[d], wo_r.at[slot], sp, partner)
        c.start()
        wofwd.append(c)
    lax.fori_loop(4, RING - 1, back, 0)
    block(RING - 1)

    for d in range(1, RING):
        remote(ssend.at[0], srecv.at[d], st_s.at[0], st_r.at[d], sp, tp).wait_recv()
    levels = [ssend[RING - 1]] + [srecv[d] for d in range(1, RING)]
    peak = levels[0]
    for v in levels[1:]:
        peak = jnp.maximum(peak, v)
    shares = [jnp.exp2(v - peak) for v in levels]
    sums = shares[0]
    for v in shares[1:]:
        sums = sums + v
    half = lax.broadcasted_iota(jnp.int32, (8, BLOCK), 0) < 4
    factor = jnp.where(half, 1.0, -lam[0]) / sums
    weights = jnp.transpose(jnp.concatenate([v * factor for v in shares] * 2, axis=0))
    for d in range(1, RING):
        remote(osend.at[0], orecv.at[d], o_s.at[0], o_r.at[d], sp, tp).wait_recv()
    mixed = jnp.zeros((BLOCK, 128), F32)
    for d in range(RING):
        u = (osend[RING - 1] if d == 0 else orecv[d]).astype(F32)
        mixed = mixed + u[:, 0:128] * weights[:, 8 * d : 8 * d + 1]
        mixed = mixed + u[:, 128:256] * weights[:, 8 * d + 4 : 8 * d + 5]
    normed = mixed * lax.rsqrt(jnp.mean(mixed * mixed, axis=1, keepdims=True) + EPSILON) * gain[...]
    hsend[...] = normed.astype(BF16).reshape(TP, ROWS, 128)
    hs = [
        remote(hsend.at[(tp + d) % TP], hrecv.at[tp], h_s.at[d], h_r.at[tp], sp, (tp + d) % TP)
        for d in range(1, TP)
    ]
    for c in hs:
        c.start()
    hrecv[tp] = hsend[tp]
    for d in range(4):
        slot = ((x + d) % 4) * 2 + 1 - core
        remote(wo.at[slot], wo.at[slot], wo_s.at[0], wo_r.at[slot], sp, tp).wait_recv()
    for d in range(1, TP):
        slot = (tp + d) % TP
        remote(hrecv.at[slot], hrecv.at[slot], h_s.at[0], h_r.at[slot], sp, tp).wait_recv()
    heads = jnp.concatenate([hrecv[j] for j in range(TP)], axis=1)
    for k in range(WIDTH // 256):
        cols = slice(k * 256, (k + 1) * 256)
        branch = dot(heads, wo[:, :, cols].reshape(TP * 128, 256))
        gate = jnp.concatenate([modv[0, 32 + 2 * k : 33 + 2 * k, :], modv[0, 33 + 2 * k : 34 + 2 * k, :]], axis=1)
        out[:, cols] = (lat[tp, :, cols].astype(F32) + gate * branch).astype(BF16)

    for c in parts + lats + wos + ys + zs + fwd + wofwd + qs + kvs + hs:
        c.wait_send()
    for k in range(RING - 1):
        remote(ssend.at[k], srecv.at[k], st_s.at[k], st_r.at[k], sp, tp).wait_send()
        remote(osend.at[k], orecv.at[k], o_s.at[k], o_r.at[k], sp, tp).wait_send()


def body(
    latent, context, condition, context_condition, modulation_weight, query_first, query_second, key_first,
    key_second, value_weight, lambda_head, context_score_boost, head_gain, output_weight,
):
    freq = jnp.asarray(np.tile(THETA ** (-np.arange(16, dtype=np.float32) / 16), 8)[None].astype(np.float32))
    vmem = pl.BlockSpec(memory_space=pltpu.VMEM)
    smem = pl.BlockSpec(memory_space=pltpu.SMEM)
    hbm = pl.BlockSpec(memory_space=pl.ANY)
    dma = pltpu.SemaphoreType.DMA
    return pl.pallas_call(
        kernel,
        out_shape=jax.ShapeDtypeStruct((ROWS, WIDTH), BF16),
        in_specs=[hbm, hbm, vmem, vmem, hbm, hbm, hbm, hbm, hbm, hbm, smem, smem, vmem, hbm, vmem],
        out_specs=vmem,
        scratch_shapes=[
            pltpu.VMEM((TP, ROWS, WIDTH), BF16),
            pltpu.VMEM((CTX, WIDTH), BF16),
            pltpu.VMEM((256, CHUNK), BF16),
            pltpu.VMEM((4, WIDTH, 64), BF16),
            pltpu.VMEM((WIDTH, 384), BF16),
            pltpu.VMEM((TP, 128, WIDTH), BF16),
            pltpu.VMEM((TP, 2, 128), F32),
            pltpu.VMEM((RING, RING, 2, 128), F32),
            pltpu.VMEM((2, 48, 128), F32),
            pltpu.VMEM((KEYS, WIDTH), BF16),
            pltpu.VMEM((BLOCK, 128), F32),
            pltpu.VMEM((BLOCK, 128), F32),
            pltpu.VMEM((RING, BLOCK, 128), BF16),
            pltpu.VMEM((RING, KEYS, 256), BF16),
            pltpu.VMEM((RING + 1, BLOCK, 256), BF16),
            pltpu.VMEM((128, 128), BF16),
            pltpu.VMEM((RING, BLOCK, 256), BF16),
            pltpu.VMEM((RING, 8, BLOCK), F32),
            pltpu.VMEM((RING, BLOCK, 256), BF16),
            pltpu.VMEM((RING, 8, BLOCK), F32),
            pltpu.VMEM((TP, ROWS, 128), BF16),
            pltpu.VMEM((TP, ROWS, 128), BF16),
            dma((9,)),
            dma((8,)), dma((8,)), dma((8,)), dma((8,)), dma((8,)), dma((8,)),
            dma((4,)), dma((8,)), dma((4,)), dma((4,)), dma((8,)), dma((4,)),
            dma((8,)), dma((8,)), dma((8,)), dma((8,)), dma((8,)), dma((8,)),
            dma((8,)), dma((8,)), dma((8,)), dma((8,)),
        ],
        compiler_params=pltpu.CompilerParams(
            collective_id=0, has_side_effects=True, vmem_limit_bytes=60 * 2**20
        ),
        name="whole",
    )(
        latent, context, condition.reshape(1, 256), context_condition.reshape(1, 256), modulation_weight,
        query_first, query_second, key_first, key_second, value_weight, lambda_head, context_score_boost,
        head_gain.reshape(1, 128), output_weight, freq,
    )


def solution(mesh):
    in_specs = (
        P(("sp", "tp"), None), P("sp", None), P("tp"), P("tp"), P("tp", "sp"), P(None, "tp"), P(None, "tp"),
        P(None, "tp"), P(None, "tp"), P(None, "tp"), P("tp"), P("tp"), P(), P("tp", None),
    )
    out_specs = P(("sp", "tp"), None)
    return jax.shard_map(body, mesh=mesh, in_specs=in_specs, out_specs=out_specs, check_vma=False)
```

time: 347 us -> 91.5 us (0.26)
  waiting for transfers between devices: 144 us -> 0 us
  Pallas kernels: 0 us -> 81.8 us
  matrix products: 60.3 us -> 0 us
  blocking collectives: 59.5 us -> 0 us
  starting transfers between devices: 27.8 us -> 0 us
  local copies, waits for them, and re-layouts: 24.6 us -> 8.13 us
  between operations: 14.9 us -> 1.31 us
  other arithmetic: 12.3 us -> 0 us
    all_gather x2 -> x0, waiting for transfers between devices: 115 us -> none  [the longest x1 79 us: body(): lax.all_gather(latent_values, 'sp', axis=0, tiled=True)]
    pallas_call x0 -> x1, Pallas kernels: none -> 81.8 us  [body(): pl.pallas_call(kernel, out_shape=jax.ShapeDtypeStruct((ROWS, WIDTH), BF16...]
    dot_general x78 -> x0, matrix products: 60.3 us -> none  [the longest x34 43.2 us: update(): jnp.einsum('hqk,khe->qhe', exp_weights.astype(jnp.bfloat16), values_heads...]
    all_gather x1 -> x0, blocking collectives: 35.7 us -> none  [in_one_piece(): out = lax.all_gather(both, axis, axis=dim, tiled=True)]
    all_to_all x3 -> x0, waiting for transfers between devices: 29.4 us -> none  [copy_for_each(): lax.all_to_all(jnp.broadcast_to(shard[None], (size, *shard.shape)), axis,...]
    all_to_all x3 -> x0, starting transfers between devices: 27.8 us -> none  [copy_for_each(): lax.all_to_all(jnp.broadcast_to(shard[None], (size, *shard.shape)), axis,...]
    all_to_all x1 -> x0, blocking collectives: 23.8 us -> none  [sum_at_owner(): lax.all_to_all(tiles, axis, split_axis=0, concat_axis=0, tiled=True)]
    squeeze x16 -> x0, local copies, waits for them, and re-layouts: 15.6 us -> none  [fold_keys(): carry, unused = lax.scan(update, carry, blocks)]
  transfers between devices with their start and end apart: 5 -> 0, of which waited for: 5 -> 0; matrix products, arithmetic and copies ran while one was open for 4% -> 0% of each run, Pallas kernels for 0% -> 0%
where the time goes in v1:
time: 91.5 us; the launch traced here: 91.3 us
  Pallas kernels  81.8 us (89%)
  local copies, waits for them, and re-layouts  8.13 us (9%)
  between operations  1.31 us (1%)
    pallas_call x1, Pallas kernels, body(): pl.pallas_call(kernel, out_shape=jax.ShapeDtypeStruct((ROWS, WIDTH), BF16...  81.8 us
    unnamed x12, local copies, waits for them, and re-layouts  8.13 us

profile of v1, /device:TPU:1, one launch (start us, length us, event | category | flops | bytes accessed | tf_op | source)
XLA Modules:
  0.0 91.3 jit_solution(7639780658753685430)
XLA Ops:
  1.3 1.5 %copy.16.modw = bf16[256,96]{1,0:T(8,128)(2,1)} copy(bf16[256,96]{0,1:T(8,128)(2,1)} %param.19) | data formatting | bytes 98304 | tf_op args[4]
  2.8 0.0 copy-start
  2.8 2.0 %copy.17.wq1 = bf16[2048,64]{1,0:T(8,128)(2,1)} copy(bf16[2048,64]{0,1:T(8,128)(2,1)} %param.20) | data formatting | bytes 524288 | tf_op args[5]
  4.8 0.0 copy-done
  4.8 0.0 copy-start.1
  4.8 1.0 %copy.18.wq2 = bf16[2048,64]{1,0:T(8,128)(2,1)} copy(bf16[2048,64]{0,1:T(8,128)(2,1)S(1)} %copy-done) | data formatting | bytes 524288 | tf_op args[6]
  5.8 0.0 copy-done.1
  5.8 0.0 copy-start.2
  5.8 1.0 %copy.19.wk1 = bf16[2048,64]{1,0:T(8,128)(2,1)} copy(bf16[2048,64]{0,1:T(8,128)(2,1)S(1)} %copy-done.1) | data formatting | bytes 524288 | tf_op args[7]
  6.9 0.0 copy-done.2
  6.9 1.0 %copy.20.wk2 = bf16[2048,64]{1,0:T(8,128)(2,1)} copy(bf16[2048,64]{0,1:T(8,128)(2,1)S(1)} %copy-done.2) | data formatting | bytes 524288 | tf_op args[8]
  7.9 81.8 %whole.1 = bf16[32,2048]{1,0:T(8,128)(2,1)} custom-call(bf16[32,2048]{1,0:T(8,128)(2,1)} %latent.1, bf16[8,2048]{1,0:T(8,128)(2,1)} %context.1, f32[1,256]{1,0:T(1,128)} %bitcast.3, f32[1,256]{1,0:T(1,128)} %bitcast.4, bf16[256,96]{1,0:T(8,128)(2,1)} %copy.16.modw, bf16[2048,64]{1,0:T(8,128)(2,1)} %copy.17.wq1, bf16[2048,64]{1,0:T(8,128)(2,1)} %copy.18.wq2, ...), custom_call_target="tpu_custom_call" | custom-call | tf_op jit(solution)/shard_map/whole/pallas_call | solution.py:332
  89.7 1.6 %copy.24 = bf16[32,2048]{1,0:T(8,128)(2,1)} copy(bf16[32,2048]{1,0:T(8,128)(2,1)} %whole.1) | data formatting | bytes 262144
Async XLA Ops:
  2.8 2.0 %copy-start = (bf16[2048,64]{0,1:T(8,128)(2,1)S(1)}, bf16[2048,64]{0,1:T(8,128)(2,1)}, u32[]{:S(2)}) copy-start(bf16[2048,64]{0,1:T(8,128)(2,1)} %param.21) | copy-start | bytes 786436
  4.8 1.0 %copy-start.1 = (bf16[2048,64]{0,1:T(8,128)(2,1)S(1)}, bf16[2048,64]{0,1:T(8,128)(2,1)}, u32[]{:S(2)}) copy-start(bf16[2048,64]{0,1:T(8,128)(2,1)} %param.22) | copy-start | bytes 786436
  5.8 1.0 %copy-start.2 = (bf16[2048,64]{0,1:T(8,128)(2,1)S(1)}, bf16[2048,64]{0,1:T(8,128)(2,1)}, u32[]{:S(2)}) copy-start(bf16[2048,64]{0,1:T(8,128)(2,1)} %param.23) | copy-start | bytes 786436

commit v2 on v1

--- a/solution.py
+++ b/solution.py
@@ -46,7 +46,7 @@
 def kernel(
     latent, context, cond, ccond, modw, wq1, wq2, wk1, wk2, wv, lam, boost, gain, wout, freq,
     out,
-    lat, ctx, mw, w64, wcat, wo, part, modg, modv, h, cosb, sinb, qb, kvb, vx, kc,
+    lat, ctx, mw, wqk, wval, wo, part, modg, modv, h, cosb, sinb, qb, kvb, vx, kc,
     osend, ssend, orecv, srecv, hsend, hrecv,
     load, part_s, part_r, y_s, y_r, z_s, z_r, lat_s, lat_r, latf_s, wo_s, wo_r, wof_s,
     q_s, q_r, kv_s, kv_r, o_s, o_r, st_s, st_r, h_s, h_r,
@@ -72,11 +72,11 @@
         pltpu.make_async_copy(latent, lat.at[tp], load.at[1]),
         pltpu.make_async_copy(context, ctx, load.at[2]),
         pltpu.make_async_copy(wout, wo.at[tp], load.at[3]),
-        pltpu.make_async_copy(wq1, w64.at[0], load.at[4]),
-        pltpu.make_async_copy(wq2, w64.at[1], load.at[5]),
-        pltpu.make_async_copy(wk1, w64.at[2], load.at[6]),
-        pltpu.make_async_copy(wk2, w64.at[3], load.at[7]),
-        pltpu.make_async_copy(wv, wcat.at[:, 256:384], load.at[8]),
+        pltpu.make_async_copy(wq1, wqk.at[0:64], load.at[4]),
+        pltpu.make_async_copy(wq2, wqk.at[64:128], load.at[5]),
+        pltpu.make_async_copy(wk1, wqk.at[128:192], load.at[6]),
+        pltpu.make_async_copy(wk2, wqk.at[192:256], load.at[7]),
+        pltpu.make_async_copy(wv, wval, load.at[8]),
     ]
     for c in loads:
         c.start()
@@ -90,7 +90,7 @@
 
     loads[0].wait()
     signal = silu(jnp.concatenate([cond[...], ccond[...], jnp.zeros((6, 256), F32)], axis=0)).astype(BF16)
-    mine = dot(signal, mw[...])[0:2]
+    mine = dot(signal, mw[...], NT)[0:2]
     part[0] = jnp.concatenate([mine, jnp.zeros((2, 128 - CHUNK), F32)], axis=1)
     loads[1].wait()
     loads[3].wait()
@@ -104,10 +104,6 @@
     lats = [remote(lat.at[tp], lat.at[tp], lat_s.at[d], lat_r.at[tp], sp, chip(d)) for d in range(1, 4)]
     lats.append(remote(lat.at[tp], lat.at[tp], lat_s.at[0], lat_r.at[tp], sp, partner))
     for c in lats:
-        c.start()
-    wos = [remote(wo.at[tp], wo.at[tp], wo_s.at[d], wo_r.at[tp], sp, chip(d)) for d in range(1, 4)]
-    wos.append(remote(wo.at[tp], wo.at[tp], wo_s.at[0], wo_r.at[tp], sp, partner))
-    for c in wos:
         c.start()
 
     for c in parts:
@@ -144,8 +140,6 @@
 
     for c in loads[4:]:
         c.wait()
-    wcat[:, 0:128] = jnp.concatenate([w64[0], w64[1]], axis=1)
-    wcat[:, 128:256] = jnp.concatenate([w64[2], w64[3]], axis=1)
     ones = jnp.ones((BLOCK, 128), BF16)
     for j in range(RING):
         vx[j, :, 128:256] = ones
@@ -189,6 +183,10 @@
         slot = ((x + d) % 4) * 2 + 1 - core
         remote(lat.at[slot], lat.at[slot], lat_s.at[0], lat_r.at[slot], sp, tp).wait_recv()
 
+    wos = [remote(wo.at[tp], wo.at[tp], wo_s.at[d], wo_r.at[tp], sp, chip(d)) for d in range(1, 4)]
+    wos.append(remote(wo.at[tp], wo.at[tp], wo_s.at[0], wo_r.at[tp], sp, partner))
+    for c in wos:
+        c.start()
     def fill(i, carry):
         v = lat[i // 2, pl.ds(pl.multiple_of((i % 2) * 16, 16), 16), :].astype(F32)
         h[pl.ds(pl.multiple_of(i * 16, 16), 16), :] = modulated(v, 0).astype(BF16)
@@ -196,17 +194,18 @@
 
     lax.fori_loop(0, BLOCK // 16, fill, 0)
 
-    qkv = dot(h[...], wcat[...])
+    qk = dot(h[...], wqk[...], NT)
+    val = dot(h[...], wval[...])
     cosine, sine = cosb[...], sinb[...]
 
     def rope(v):
         turned = jnp.where(lane % 32 < 16, pltpu.roll(v, 112, 1), pltpu.roll(v, 16, 1))
         return v * cosine + turned * sine
 
-    qb[0] = (rope(qkv[0:BLOCK, 0:128]) * (LOG2E / 8.0)).astype(BF16)
-    kvb[0, 0:BLOCK, 0:128] = rope(qkv[0:BLOCK, 128:256]).astype(BF16)
-    kvb[0, BLOCK:KEYS, 0:128] = qkv[BLOCK:KEYS, 128:256].astype(BF16)
-    kvb[0, :, 128:256] = qkv[:, 256:384].astype(BF16)
+    qb[0] = (rope(qk[0:BLOCK, 0:128]) * (LOG2E / 8.0)).astype(BF16)
+    kvb[0, 0:BLOCK, 0:128] = rope(qk[0:BLOCK, 128:256]).astype(BF16)
+    kvb[0, BLOCK:KEYS, 0:128] = qk[BLOCK:KEYS, 128:256].astype(BF16)
+    kvb[0, :, 128:256] = val.astype(BF16)
 
     kvs = [
         remote(kvb.at[0], kvb.at[d], kv_s.at[d], kv_r.at[d], at_b((b + d) % RING), tp) for d in range(1, RING)
@@ -337,9 +336,9 @@
         scratch_shapes=[
             pltpu.VMEM((TP, ROWS, WIDTH), BF16),
             pltpu.VMEM((CTX, WIDTH), BF16),
-            pltpu.VMEM((256, CHUNK), BF16),
-            pltpu.VMEM((4, WIDTH, 64), BF16),
-            pltpu.VMEM((WIDTH, 384), BF16),
+            pltpu.VMEM((CHUNK, 256), BF16),
+            pltpu.VMEM((256, WIDTH), BF16),
+            pltpu.VMEM((WIDTH, 128), BF16),
             pltpu.VMEM((TP, 128, WIDTH), BF16),
             pltpu.VMEM((TP, 2, 128), F32),
             pltpu.VMEM((RING, RING, 2, 128), F32),
@@ -368,8 +367,8 @@
         ),
         name="whole",
     )(
-        latent, context, condition.reshape(1, 256), context_condition.reshape(1, 256), modulation_weight,
-        query_first, query_second, key_first, key_second, value_weight, lambda_head, context_score_boost,
+        latent, context, condition.reshape(1, 256), context_condition.reshape(1, 256), modulation_weight.T,
+        query_first.T, query_second.T, key_first.T, key_second.T, value_weight, lambda_head, context_score_boost,
         head_gain.reshape(1, 128), output_weight, freq,
     )
 

time: 91.5 us -> 77.9 us (0.85)
  Pallas kernels: 81.8 us -> 74.8 us
  local copies, waits for them, and re-layouts: 8.13 us -> 1.57 us
    pallas_call x1, Pallas kernels: 81.8 us -> 74.8 us  [body(): pl.pallas_call(kernel, out_shape=jax.ShapeDtypeStruct((ROWS, WIDTH), BF16...]
    unnamed x12 -> x1, local copies, waits for them, and re-layouts: 8.13 us -> 1.57 us
where the time goes in v2:
time: 77.9 us; the launch traced here: 77.7 us
  Pallas kernels  74.8 us (96%)
  local copies, waits for them, and re-layouts  1.57 us (2%)
  between operations  1.3 us (2%)
    pallas_call x1, Pallas kernels, body(): pl.pallas_call(kernel, out_shape=jax.ShapeDtypeStruct((ROWS, WIDTH), BF16...  74.8 us
    unnamed x1, local copies, waits for them, and re-layouts  1.57 us

profile of v2, /device:TPU:1, one launch (start us, length us, event | category | flops | bytes accessed | tf_op | source)
XLA Modules:
  0.0 77.7 jit_solution(4773192008983929926)
XLA Ops:
  1.3 74.8 %whole.1 = bf16[32,2048]{1,0:T(8,128)(2,1)} custom-call(bf16[32,2048]{1,0:T(8,128)(2,1)} %latent.1, bf16[8,2048]{1,0:T(8,128)(2,1)} %context.1, f32[1,256]{1,0:T(1,128)} %bitcast.13, f32[1,256]{1,0:T(1,128)} %bitcast.14, bf16[96,256]{1,0:T(8,128)(2,1)} %bitcast.12, bf16[64,2048]{1,0:T(8,128)(2,1)} %bitcast.8, bf16[64,2048]{1,0:T(8,128)(2,1)} %bitcast.9, ...), custom_call_target="tpu_custom_call" | custom-call | tf_op jit(solution)/shard_map/whole/pallas_call | solution.py:331
  76.1 1.6 %copy.19 = bf16[32,2048]{1,0:T(8,128)(2,1)} copy(bf16[32,2048]{1,0:T(8,128)(2,1)} %whole.1) | data formatting | bytes 262144

commit v3 on v2

v3 whole, which is shorter than its diff:
```python
import functools
import math

import jax
import jax.numpy as jnp
import numpy as np
from jax import lax
from jax.experimental import pallas as pl
from jax.experimental.pallas import tpu as pltpu
from jax.sharding import PartitionSpec as P

MESH = pl.DeviceIdType.MESH
EPSILON = 1e-06
THETA = 10000.0
GRID_W = 64
RING = 8
TP = 8
ROWS = 32
BLOCK = 256
CTX = 8
KEYS = BLOCK + 2 * CTX
WIDTH = 2048
CHUNK = 96
LOG2E = math.log2(math.e)
BF16 = jnp.bfloat16
F32 = jnp.float32

NT = (((1,), (1,)), ((), ()))
NN = (((1,), (0,)), ((), ()))


def dot(a, b, dims=NN):
    return lax.dot_general(a, b, dims, preferred_element_type=F32)


def remote(src, dst, send, recv, sp, tp):
    return pltpu.make_async_remote_copy(
        src_ref=src, dst_ref=dst, send_sem=send, recv_sem=recv, device_id=(sp, tp), device_id_type=MESH
    )


def silu(v):
    return v / (1.0 + jnp.exp(-v))


def kernel(
    latent, context, cond_in, ccond_in, modw, wq1, wq2, wk1, wk2, wv, lam_in, boost_in, gain_in, wout, freq_in,
    out,
    cond, ccond, gain, freq, lam, boost, rows_out,
    lat, ctx, mw, wqk, wval, wo, part, modg, modv, nlat, nctx, cosb, sinb, qb, kb, vb, vx, kc,
    held, top, osend, ssend, orecv, srecv, hsend, hrecv,
    load, store, part_s, part_r, z_s, z_r, lat_s, lat_r, wo_s, wo_r, wo2_r,
    q_s, q_r, k_s, k_r, v_s, v_r, o_s, o_r, st_s, st_r, h_s, h_r,
):
    sp, tp = lax.axis_index("sp"), lax.axis_index("tp")
    z, y = sp // RING, sp % RING
    x, core = tp // 2, tp % 2
    partner = x * 2 + 1 - core
    a = core * z + (1 - core) * y
    b = core * y + (1 - core) * z

    def at_a(i):
        return (1 - core) * (z * RING + i) + core * (i * RING + y)

    def at_b(i):
        return (1 - core) * (i * RING + y) + core * (z * RING + i)

    def chip(d):
        return ((x + d) % 4) * 2 + core

    loads = [
        pltpu.make_async_copy(modw, mw, load.at[0]),
        pltpu.make_async_copy(latent, lat.at[tp], load.at[1]),
        pltpu.make_async_copy(context, ctx, load.at[2]),
        pltpu.make_async_copy(wout, wo.at[tp], load.at[3]),
        pltpu.make_async_copy(wq1, wqk.at[0:64], load.at[4]),
        pltpu.make_async_copy(wq2, wqk.at[64:128], load.at[5]),
        pltpu.make_async_copy(wk1, wqk.at[128:192], load.at[6]),
        pltpu.make_async_copy(wk2, wqk.at[192:256], load.at[7]),
        pltpu.make_async_copy(wv, wval, load.at[8]),
        pltpu.make_async_copy(freq_in, freq, load.at[9]),
        pltpu.make_async_copy(gain_in, gain, load.at[10]),
        pltpu.make_async_copy(lam_in, lam, load.at[11]),
        pltpu.make_async_copy(boost_in, boost, load.at[12]),
        pltpu.make_async_copy(cond_in, cond, load.at[13]),
        pltpu.make_async_copy(ccond_in, ccond, load.at[14]),
    ]
    for c in loads:
        c.start()

    barrier = pltpu.get_barrier_semaphore()

    beside = [z * RING + (y + d) % RING for d in range(RING)]
    across = [(tp + d) % TP for d in range(TP)]
    for n in range(1, TP * RING):
        pl.semaphore_signal(barrier, inc=1, device_id=(beside[n // TP], across[n % TP]), device_id_type=MESH)
    for d in range(1, RING):
        pl.semaphore_signal(barrier, inc=1, device_id=(((z + d) % RING) * RING + y, tp), device_id_type=MESH)

    loads[0].wait()
    loads[13].wait()
    loads[14].wait()
    signal = silu(jnp.concatenate([cond[...], ccond[...], jnp.zeros((6, 256), F32)], axis=0)).astype(BF16)
    mine = dot(signal, mw[...], NT)[0:2]
    part[0] = jnp.concatenate([mine, jnp.zeros((2, 128 - CHUNK), F32)], axis=1)
    loads[1].wait()
    loads[3].wait()
    pl.semaphore_wait(barrier, TP * RING - 1 + RING - 1)

    for n in range(1, TP * RING):
        remote(part.at[0], part.at[n], part_s, part_r, beside[n // TP], across[n % TP]).start()
    lats = [remote(lat.at[tp], lat.at[tp], lat_s, lat_r.at[tp], sp, chip(d)) for d in range(1, 4)]
    lats.append(remote(lat.at[tp], lat.at[tp], lat_s, lat_r.at[tp], sp, partner))
    for c in lats:
        c.start()

    loads[9].wait()
    row = lax.broadcasted_iota(jnp.int32, (BLOCK, 128), 0)
    lane = lax.broadcasted_iota(jnp.int32, (BLOCK, 128), 1)
    token = row + sp * BLOCK
    grid_row = token // GRID_W
    where = jnp.where(lane % 64 < 32, grid_row, token - grid_row * GRID_W).astype(F32)
    angle = where * freq[...]
    cosb[...] = jnp.cos(angle)
    sinb[...] = jnp.where(lane % 32 < 16, -jnp.sin(angle), jnp.sin(angle))

    others = part.at[1 : TP * RING]
    remote(others, others, part_s, part_r, sp, tp).wait_recv()
    for d in range(RING):
        total = part[d * TP]
        for n in range(1, TP):
            total = total + part[d * TP + n]
        modg[z, (y + RING - d) % RING] = total
    zs = [
        remote(modg.at[z], modg.at[z], z_s, z_r, ((z + d) % RING) * RING + y, tp)
        for d in range(1, RING)
    ]
    for c in zs:
        c.start()

    for c in loads[4:9] + loads[10:13]:
        c.wait()
    ones = jnp.ones((BLOCK, 128), BF16)
    for j in range(RING):
        vx[j, :, 128:256] = ones
    vx[RING, :, 128:256] = ones
    for d in range(1, 4):
        slot = chip(d)
        remote(lat.at[slot], lat.at[slot], lat_s, lat_r.at[slot], sp, tp).wait_recv()
        remote(lat.at[slot], lat.at[slot], lat_s, lat_r.at[slot], sp, partner).start()

    wos = [remote(wo.at[tp], wo.at[tp], wo_s, wo_r.at[tp], sp, chip(d)) for d in (1, 3)]
    wos.append(remote(wo.at[tp], wo.at[tp], wo_s, wo_r.at[tp], sp, partner))
    for c in wos:
        c.start()
    for d in range(4):
        slot = ((x + d) % 4) * 2 + 1 - core
        remote(lat.at[slot], lat.at[slot], lat_s, lat_r.at[slot], sp, tp).wait_recv()
    loads[2].wait()

    def norm(v):
        return v * lax.rsqrt(jnp.mean(v * v, axis=1, keepdims=True) + EPSILON)

    nctx[...] = norm(ctx[...].astype(F32))

    def norm_rows(i, carry):
        rows = pl.ds(pl.multiple_of(i * ROWS, ROWS), ROWS)
        nlat[rows, :] = norm(lat[i].astype(F32))
        return carry

    lax.fori_loop(0, TP, norm_rows, 0)
    far_rows = modg.at[0 : RING - 1]
    remote(far_rows, far_rows, z_s, z_r, sp, tp).wait_recv()

    lane2 = lax.broadcasted_iota(jnp.int32, (2, 128), 1)
    for g in range(16):
        c0, c1, c2, c3 = [modg[g // 2, (g % 2) * 4 + j] for j in range(4)]
        c1, c2, c3 = pltpu.roll(c1, 96, 1), pltpu.roll(c2, 64, 1), pltpu.roll(c3, 32, 1)
        rows = [jnp.where(lane2 < 96, c0, c1), jnp.where(lane2 < 64, c1, c2), jnp.where(lane2 < 32, c2, c3)]
        for m in range(3):
            for r in range(2):
                modv[r, 3 * g + m : 3 * g + m + 1, :] = rows[m][r : r + 1]

    qk, val = None, None
    pad = jnp.zeros((CTX, 256), F32)
    for c in range(WIDTH // 256):
        cols = slice(c * 256, (c + 1) * 256)
        pieces = []
        for r, n in ((0, nlat), (1, nctx)):
            scale = jnp.concatenate([modv[r, 16 + 2 * c : 17 + 2 * c, :], modv[r, 17 + 2 * c : 18 + 2 * c, :]], axis=1)
            shift = jnp.concatenate([modv[r, 2 * c : 2 * c + 1, :], modv[r, 2 * c + 1 : 2 * c + 2, :]], axis=1)
            pieces.append(n[:, cols] * (1.0 + scale) + shift)
        h = jnp.concatenate(pieces + [pad], axis=0).astype(BF16)
        one, two = dot(h, wqk[:, cols], NT), dot(h, wval[cols, :])
        qk, val = (one, two) if qk is None else (qk + one, val + two)
    cosine, sine = cosb[...], sinb[...]

    def rope(v):
        turned = jnp.where(lane % 32 < 16, pltpu.roll(v, 112, 1), pltpu.roll(v, 16, 1))
        return v * cosine + turned * sine

    def pass_on(src, dst, send, recv, to):
        remote(src, dst, send, recv, to, tp).start()

    a_up, a_down = at_a((a + 1) % RING), at_a((a + RING - 1) % RING)
    b_up, b_down = at_b((b + 1) % RING), at_b((b + RING - 1) % RING)

    def cut(buf, slot, c):
        if buf.shape[1] == BLOCK:
            return buf.at[slot, c * 128 : (c + 1) * 128]
        return buf.at[slot, 144 * c : 144 + 128 * c]

    def pass_query(near, far, c):
        to = a_up if far + c < 5 else a_down
        pass_on(cut(qb, near, c), cut(qb, far, c), q_s, q_r.at[c, far], to)

    def pass_key(near, far, c):
        pass_on(cut(kb, near, c), cut(kb, far, c), k_s, k_r.at[c, far], b_up if far < 5 else b_down)

    def pass_value(near, far, c):
        pass_on(cut(vb, near, c), cut(vb, far, c), v_s, v_r.at[c, far], b_up if far < 4 else b_down)

    def arrived(buf, recv, slot, c):
        here = cut(buf, slot, c)
        remote(here, here, q_s, recv.at[c, slot], sp, tp).wait_recv()

    qb[0] = (rope(qk[0:BLOCK, 0:128]) * (LOG2E / 8.0)).astype(BF16)
    kb[0, 0:BLOCK, :] = rope(qk[0:BLOCK, 128:256]).astype(BF16)
    kb[0, BLOCK:KEYS, :] = qk[BLOCK:KEYS, 128:256].astype(BF16)
    vb[0] = val.astype(BF16)
    for c in range(2):
        for slot in (1, 7):
            pass_query(0, slot, c)
            pass_key(0, slot, c)
            pass_value(0, slot, c)
    def ring_step(pairs):
        for c in range(2):
            for near, far in pairs:
                arrived(qb, q_r, near, c)
                pass_query(near, far, c)
            for near, far in pairs:
                arrived(kb, k_r, near, c)
                pass_key(near, far, c)
            for near, far in pairs:
                arrived(vb, v_r, near, c)
                pass_value(near, far, c)

    ring_step(((1, 2), (7, 6)))

    lane1 = lax.broadcasted_iota(jnp.int32, (1, 128), 1)
    bias = jnp.where(lane1 % 16 < CTX, boost[0] * LOG2E, -1e30)

    def attend(query, slots, with_context, before):
        scores = [dot(query, kb[j, 0:BLOCK, :], NT) for j in slots]
        peak = scores[0]
        for s in scores[1:]:
            peak = jnp.maximum(peak, s)
        peak = jnp.maximum(peak[:, 0:128], peak[:, 128:256])
        if with_context:
            extra = dot(query, kc[...], NT) + bias
            peak = jnp.maximum(peak, extra)
        if before is not None:
            peak = jnp.maximum(peak, before[1])
        peak = jnp.max(peak, axis=1, keepdims=True)
        acc = None
        if before is not None:
            fade = jnp.exp2(before[1] - peak)
            acc = before[0] * jnp.concatenate([fade, fade], axis=1)
        terms = [(s, vx[j]) for j, s in zip(slots, scores)]
        if with_context:
            terms.append((extra, vx[RING, 0:128, :]))
        for s, v in terms:
            term = dot(jnp.exp2(s - peak).astype(BF16), v)
            acc = term if acc is None else acc + term
        return acc, jnp.broadcast_to(peak, (BLOCK, 128))

    def work(slot, slots, with_context=False, again=False):
        query = qb[slot]
        none = jnp.zeros_like(query)
        for m in range(2):
            masked = jnp.where(lane < 64, query, none) if m == 0 else jnp.where(lane < 64, none, query)
            before = (held[slot, m], top[slot, m]) if again else None
            held[slot, m], top[slot, m] = attend(masked, slots, with_context, before)

    def take_in(slot, box):
        remote(ssend.at[0], srecv.at[box], st_s, st_r.at[box], sp, tp).wait_recv()
        remote(osend.at[0], orecv.at[box], o_s, o_r.at[box], sp, tp).wait_recv()
        theirs = jnp.transpose(jnp.concatenate([srecv[box]] * 16, axis=0))
        for m in range(2):
            mine = top[slot, m]
            their_top = theirs[:, 4 * m : 4 * m + 1]
            new = jnp.maximum(mine, their_top)
            up, down = jnp.exp2(mine - new), jnp.exp2(their_top - new)
            now = held[slot, m]
            held[slot, m, :, 0:128] = now[:, 0:128] * up + orecv[box, :, m * 128 : (m + 1) * 128].astype(F32) * down
            held[slot, m, :, 128:256] = now[:, 128:256] * up + theirs[:, 4 * m + 2 : 4 * m + 3] * down
            top[slot, m] = new

    def stats(slot):
        where = lane % 8
        one = jnp.where(where < 2, top[slot, 0], held[slot, 0, :, 128:256])
        two = jnp.where(where < 6, top[slot, 1], held[slot, 1, :, 128:256])
        return jnp.transpose(jnp.where(where < 4, one, two))[0:8, :]

    def send_off(slot, box, to):
        osend[slot, :, 0:128] = held[slot, 0, :, 0:128].astype(BF16)
        osend[slot, :, 128:256] = held[slot, 1, :, 0:128].astype(BF16)
        ssend[slot] = stats(slot)
        to = at_a((a + to) % RING)
        remote(osend.at[slot], orecv.at[box], o_s, o_r.at[box], to, tp).start()
        remote(ssend.at[slot], srecv.at[box], st_s, st_r.at[box], to, tp).start()

    def unpack(slots):
        for j in slots:
            vx[j, :, 0:128] = vb[j, 0:BLOCK]

    unpack((0, 1, 7))
    work(0, (0, 1, 7))
    work(1, (0, 1, 7))
    ring_step(((2, 3), (6, 5)))

    def share(d):
        remote(wo.at[chip(d)], wo.at[chip(d)], wo_s, wo_r.at[chip(d)], sp, partner).start()

    for c, d in ((0, 3), (1, 1)):
        slot = chip(d)
        remote(wo.at[slot], wo.at[slot], wo_s, wo_r.at[slot], sp, tp).wait_recv()
        piece = wo.at[slot, c * 64 : (c + 1) * 64]
        remote(piece, piece, wo_s, wo2_r.at[c], sp, chip(4 - d)).start()
    share(3)
    unpack((2, 6))
    for slot in (7, 2, 6):
        work(slot, (0, 1, 7, 2, 6))
    for c in range(2):
        arrived(qb, q_r, 3, c)
        arrived(qb, q_r, 5, c)
        pass_query(3 if c == 0 else 5, 4, c)
        arrived(kb, k_r, 3, c)
        pass_key(3, 4, c)
        arrived(vb, v_r, 5, c)
        pass_value(5, 4, c)
        arrived(kb, k_r, 5, c)
        arrived(vb, v_r, 3, c)
    share(1)
    unpack((3, 5))
    for slot in (5, 3):
        work(slot, (0, 1, 7, 2, 6, 3, 5))
    for c in range(2):
        arrived(qb, q_r, 4, c)
        arrived(kb, k_r, 4, c)
        arrived(vb, v_r, 4, c)
    unpack((4,))
    for j in range(RING):
        kc[j * 16 : (j + 1) * 16, :] = kb[j, BLOCK:KEYS]
        vx[RING, j * 16 : (j + 1) * 16, 0:128] = vb[j, BLOCK:KEYS]
    work(4, tuple(range(RING)), True)
    send_off(4, 3, 7)
    work(5, (4,), True, True)
    send_off(5, 5, 1)
    work(2, (3, 5, 4), True, True)
    send_off(2, 2, 6)
    work(3, (4,), True, True)
    take_in(3, 3)
    send_off(3, 4, 5)
    work(6, (3, 5, 4), True, True)
    take_in(6, 5)
    send_off(6, 6, 2)
    for c in range(2):
        piece = wo.at[chip(2), c * 64 : (c + 1) * 64]
        remote(piece, piece, wo_s, wo2_r.at[c], sp, tp).wait_recv()
    share(2)
    work(1, (2, 6, 3, 5, 4), True, True)
    send_off(1, 1, 7)
    work(7, (3, 5, 4), True, True)
    send_off(7, 7, 1)
    work(0, (2, 6, 3, 5, 4), True, True)

    boxes = (7, 2, 1, 6, 4)
    for d in boxes:
        remote(ssend.at[0], srecv.at[d], st_s, st_r.at[d], sp, tp).wait_recv()
    levels = [stats(0)] + [srecv[d] for d in boxes]
    peak = levels[0]
    for v in levels[1:]:
        peak = jnp.maximum(peak, v)
    shares = [jnp.exp2(v - peak) for v in levels]
    sums = None
    for v, share in zip(levels, shares):
        term = share * pltpu.roll(v, 6, 0)
        sums = term if sums is None else sums + term
    first_half = lax.broadcasted_iota(jnp.int32, (8, BLOCK), 0) < 4
    factor = jnp.where(first_half, 1.0, -lam[0]) / sums
    rows = [v * factor for v in shares]
    weights = jnp.transpose(jnp.concatenate(rows + rows[0:1] * 10, axis=0))
    for d in boxes:
        remote(osend.at[0], orecv.at[d], o_s, o_r.at[d], sp, tp).wait_recv()
    mixed = jnp.zeros((BLOCK, 128), F32)
    for n, d in enumerate((0,) + boxes):
        for m in range(2):
            u = held[0, m, :, 0:128] if n == 0 else orecv[d, :, m * 128 : (m + 1) * 128].astype(F32)
            mixed = mixed + u * weights[:, 8 * n + 4 * m : 8 * n + 4 * m + 1]
    normed = mixed * lax.rsqrt(jnp.mean(mixed * mixed, axis=1, keepdims=True) + EPSILON) * gain[...]
    hsend[...] = normed.astype(BF16).reshape(TP, ROWS, 128)
    hs = [
        remote(hsend.at[(tp + d) % TP], hrecv.at[tp], h_s, h_r, sp, (tp + d) % TP)
        for d in range(1, TP)
    ]
    for c in hs:
        c.start()
    hrecv[tp] = hsend[tp]
    for d in range(4):
        slot = ((x + d) % 4) * 2 + 1 - core
        remote(wo.at[slot], wo.at[slot], wo_s, wo_r.at[slot], sp, tp).wait_recv()
    rest = hrecv.at[0 : TP - 1]
    remote(rest, rest, h_s, h_r, sp, tp).wait_recv()
    heads = jnp.concatenate([hrecv[j] for j in range(TP)], axis=1)
    for k in range(WIDTH // 256):
        cols = slice(k * 256, (k + 1) * 256)
        branch = dot(heads, wo[:, :, cols].reshape(TP * 128, 256))
        gate = jnp.concatenate([modv[0, 32 + 2 * k : 33 + 2 * k, :], modv[0, 33 + 2 * k : 34 + 2 * k, :]], axis=1)
        rows_out[:, cols] = (lat[tp, :, cols].astype(F32) + gate * branch).astype(BF16)
        pltpu.make_async_copy(rows_out.at[:, cols], out.at[:, cols], store).start()

    for sent, sem in (
        (others, part_s), (lat.at[1:8], lat_s), (wo.at[1:8], wo_s), (far_rows, z_s), (qb.at[1:8], q_s), (kb.at[1:8], k_s),
        (vb.at[1:8], v_s), (osend.at[1:8], o_s), (ssend.at[1:8], st_s), (rest, h_s),
    ):
        remote(sent, sent, sem, part_r, sp, tp).wait_send()
    pltpu.make_async_copy(rows_out, out, store).wait()


def body(
    latent, context, condition, context_condition, modulation_weight, query_first, query_second, key_first,
    key_second, value_weight, lambda_head, context_score_boost, head_gain, output_weight,
):
    freq = jnp.asarray(np.tile(THETA ** (-np.arange(16, dtype=np.float32) / 16), 8)[None].astype(np.float32))
    hbm = pl.BlockSpec(memory_space=pl.ANY)
    dma = pltpu.SemaphoreType.DMA
    return pl.pallas_call(
        kernel,
        out_shape=jax.ShapeDtypeStruct((ROWS, WIDTH), BF16),
        in_specs=[hbm] * 15,
        out_specs=hbm,
        scratch_shapes=[
            pltpu.VMEM((1, 256), F32),
            pltpu.VMEM((1, 256), F32),
            pltpu.VMEM((1, 128), F32),
            pltpu.VMEM((1, 128), F32),
            pltpu.SMEM((1,), F32),
            pltpu.SMEM((1,), F32),
            pltpu.VMEM((ROWS, WIDTH), BF16),
            pltpu.VMEM((TP, ROWS, WIDTH), BF16),
            pltpu.VMEM((CTX, WIDTH), BF16),
            pltpu.VMEM((CHUNK, 256), BF16),
            pltpu.VMEM((256, WIDTH), BF16),
            pltpu.VMEM((WIDTH, 128), BF16),
            pltpu.VMEM((TP, 128, WIDTH), BF16),
            pltpu.VMEM((TP * RING, 2, 128), F32),
            pltpu.VMEM((RING, RING, 2, 128), F32),
            pltpu.VMEM((2, 48, 128), F32),
            pltpu.VMEM((BLOCK, WIDTH), F32),
            pltpu.VMEM((CTX, WIDTH), F32),
            pltpu.VMEM((BLOCK, 128), F32),
            pltpu.VMEM((BLOCK, 128), F32),
            pltpu.VMEM((RING, BLOCK, 128), BF16),
            pltpu.VMEM((RING, KEYS, 128), BF16),
            pltpu.VMEM((RING, KEYS, 128), BF16),
            pltpu.VMEM((RING + 1, BLOCK, 256), BF16),
            pltpu.VMEM((128, 128), BF16),
            pltpu.VMEM((RING, 2, BLOCK, 256), F32),
            pltpu.VMEM((RING, 2, BLOCK, 128), F32),
            pltpu.VMEM((RING, BLOCK, 256), BF16),
            pltpu.VMEM((RING, 8, BLOCK), F32),
            pltpu.VMEM((RING, BLOCK, 256), BF16),
            pltpu.VMEM((RING, 8, BLOCK), F32),
            pltpu.VMEM((TP, ROWS, 128), BF16),
            pltpu.VMEM((TP, ROWS, 128), BF16),
            dma((15,)), dma(()), dma(()), dma(()), dma(()), dma(()), dma(()), dma((8,)), dma(()), dma((8,)), dma((2,)),
            dma(()), dma((2, 8)), dma(()), dma((2, 8)), dma(()), dma((2, 8)),
            dma(()), dma((8,)), dma(()), dma((8,)), dma(()), dma(()),
        ],
        compiler_params=pltpu.CompilerParams(
            collective_id=0, has_side_effects=True, vmem_limit_bytes=60 * 2**20
        ),
        name="whole",
    )(
        latent, context, condition.reshape(1, 256), context_condition.reshape(1, 256), modulation_weight.T,
        query_first.T, query_second.T, key_first.T, key_second.T, value_weight, lambda_head, context_score_boost,
        head_gain.reshape(1, 128), output_weight, freq,
    )


def solution(mesh):
    in_specs = (
        P(("sp", "tp"), None), P("sp", None), P("tp"), P("tp"), P("tp", "sp"), P(None, "tp"), P(None, "tp"),
        P(None, "tp"), P(None, "tp"), P(None, "tp"), P("tp"), P("tp"), P(), P("tp", None),
    )
    out_specs = P(("sp", "tp"), None)
    return jax.shard_map(body, mesh=mesh, in_specs=in_specs, out_specs=out_specs, check_vma=False)
```

time: 77.9 us -> 72.9 us (0.936)
  Pallas kernels: 74.8 us -> 69.8 us
    pallas_call x1, Pallas kernels: 74.8 us -> 69.8 us  [body(): pl.pallas_call(kernel, out_shape=jax.ShapeDtypeStruct((ROWS, WIDTH), BF16...]
where the time goes in v3:
time: 72.9 us; the launch traced here: 72.7 us
  Pallas kernels  69.8 us (96%)
  local copies, waits for them, and re-layouts  1.57 us (2%)
  between operations  1.31 us (2%)
    pallas_call x1, Pallas kernels, body(): pl.pallas_call(kernel, out_shape=jax.ShapeDtypeStruct((ROWS, WIDTH), BF16...  69.8 us
    unnamed x1, local copies, waits for them, and re-layouts  1.57 us

profile of v3, /device:TPU:1, one launch (start us, length us, event | category | flops | bytes accessed | tf_op | source)
XLA Modules:
  0.0 72.7 jit_solution(41236232479159405)
XLA Ops:
  1.3 69.8 %whole.1 = bf16[32,2048]{1,0:T(8,128)(2,1)} custom-call(bf16[32,2048]{1,0:T(8,128)(2,1)} %latent.1, bf16[8,2048]{1,0:T(8,128)(2,1)} %context.1, f32[1,256]{1,0:T(1,128)} %bitcast.13, f32[1,256]{1,0:T(1,128)} %bitcast.14, bf16[96,256]{1,0:T(8,128)(2,1)} %bitcast.12, bf16[64,2048]{1,0:T(8,128)(2,1)} %bitcast.8, bf16[64,2048]{1,0:T(8,128)(2,1)} %bitcast.9, ...), custom_call_target="tpu_custom_call" | custom-call | tf_op jit(solution)/shard_map/whole/pallas_call | solution.py:438
  71.1 1.6 %copy.19 = bf16[32,2048]{1,0:T(8,128)(2,1)} copy(bf16[32,2048]{1,0:T(8,128)(2,1)} %whole.1) | data formatting | bytes 262144

commit v4 on v3

--- a/solution.py
+++ b/solution.py
@@ -46,10 +46,10 @@
 def kernel(
     latent, context, cond_in, ccond_in, modw, wq1, wq2, wk1, wk2, wv, lam_in, boost_in, gain_in, wout, freq_in,
     out,
-    cond, ccond, gain, freq, lam, boost, rows_out,
+    cond, ccond, gain, freq, lam, boost,
     lat, ctx, mw, wqk, wval, wo, part, modg, modv, nlat, nctx, cosb, sinb, qb, kb, vb, vx, kc,
     held, top, osend, ssend, orecv, srecv, hsend, hrecv,
-    load, store, part_s, part_r, z_s, z_r, lat_s, lat_r, wo_s, wo_r, wo2_r,
+    load, part_s, part_r, z_s, z_r, lat_s, lat_r, wo_s, wo_r, wo2_r,
     q_s, q_r, k_s, k_r, v_s, v_r, o_s, o_r, st_s, st_r, h_s, h_r,
 ):
     sp, tp = lax.axis_index("sp"), lax.axis_index("tp")
@@ -153,22 +153,28 @@
     wos.append(remote(wo.at[tp], wo.at[tp], wo_s, wo_r.at[tp], sp, partner))
     for c in wos:
         c.start()
+    loads[2].wait()
+
+    def norm(v):
+        return v * lax.rsqrt(jnp.mean(v * v, axis=1, keepdims=True) + EPSILON)
+
+    def norm_rows(slot):
+        nlat[pl.ds(pl.multiple_of(slot * ROWS, ROWS), ROWS), :] = norm(lat[slot].astype(F32))
+
+    def norm_mine(i, carry):
+        norm_rows(i * 2 + core)
+        return carry
+
+    def norm_partner(i, carry):
+        norm_rows(i * 2 + 1 - core)
+        return carry
+
+    nctx[...] = norm(ctx[...].astype(F32))
+    lax.fori_loop(0, TP // 2, norm_mine, 0)
     for d in range(4):
         slot = ((x + d) % 4) * 2 + 1 - core
         remote(lat.at[slot], lat.at[slot], lat_s, lat_r.at[slot], sp, tp).wait_recv()
-    loads[2].wait()
-
-    def norm(v):
-        return v * lax.rsqrt(jnp.mean(v * v, axis=1, keepdims=True) + EPSILON)
-
-    nctx[...] = norm(ctx[...].astype(F32))
-
-    def norm_rows(i, carry):
-        rows = pl.ds(pl.multiple_of(i * ROWS, ROWS), ROWS)
-        nlat[rows, :] = norm(lat[i].astype(F32))
-        return carry
-
-    lax.fori_loop(0, TP, norm_rows, 0)
+    lax.fori_loop(0, TP // 2, norm_partner, 0)
     far_rows = modg.at[0 : RING - 1]
     remote(far_rows, far_rows, z_s, z_r, sp, tp).wait_recv()
 
@@ -354,28 +360,28 @@
         kc[j * 16 : (j + 1) * 16, :] = kb[j, BLOCK:KEYS]
         vx[RING, j * 16 : (j + 1) * 16, 0:128] = vb[j, BLOCK:KEYS]
     work(4, tuple(range(RING)), True)
-    send_off(4, 3, 7)
-    work(5, (4,), True, True)
-    send_off(5, 5, 1)
+    send_off(4, 3, 1)
+    work(3, (4,), True, True)
+    send_off(3, 4, 5)
     work(2, (3, 5, 4), True, True)
     send_off(2, 2, 6)
-    work(3, (4,), True, True)
-    take_in(3, 3)
-    send_off(3, 4, 5)
-    work(6, (3, 5, 4), True, True)
-    take_in(6, 5)
-    send_off(6, 6, 2)
+    work(5, (4,), True, True)
+    take_in(5, 3)
+    send_off(5, 5, 1)
+    work(1, (2, 6, 3, 5, 4), True, True)
+    send_off(1, 1, 7)
+    work(7, (3, 5, 4), True, True)
+    send_off(7, 7, 1)
     for c in range(2):
         piece = wo.at[chip(2), c * 64 : (c + 1) * 64]
         remote(piece, piece, wo_s, wo2_r.at[c], sp, tp).wait_recv()
     share(2)
-    work(1, (2, 6, 3, 5, 4), True, True)
-    send_off(1, 1, 7)
-    work(7, (3, 5, 4), True, True)
-    send_off(7, 7, 1)
+    work(6, (3, 5, 4), True, True)
+    take_in(6, 5)
+    send_off(6, 6, 2)
     work(0, (2, 6, 3, 5, 4), True, True)
 
-    boxes = (7, 2, 1, 6, 4)
+    boxes = (2, 4, 1, 7, 6)
     for d in boxes:
         remote(ssend.at[0], srecv.at[d], st_s, st_r.at[d], sp, tp).wait_recv()
     levels = [stats(0)] + [srecv[d] for d in boxes]
@@ -417,15 +423,13 @@
         cols = slice(k * 256, (k + 1) * 256)
         branch = dot(heads, wo[:, :, cols].reshape(TP * 128, 256))
         gate = jnp.concatenate([modv[0, 32 + 2 * k : 33 + 2 * k, :], modv[0, 33 + 2 * k : 34 + 2 * k, :]], axis=1)
-        rows_out[:, cols] = (lat[tp, :, cols].astype(F32) + gate * branch).astype(BF16)
-        pltpu.make_async_copy(rows_out.at[:, cols], out.at[:, cols], store).start()
+        out[:, cols] = (lat[tp, :, cols].astype(F32) + gate * branch).astype(BF16)
 
     for sent, sem in (
         (others, part_s), (lat.at[1:8], lat_s), (wo.at[1:8], wo_s), (far_rows, z_s), (qb.at[1:8], q_s), (kb.at[1:8], k_s),
         (vb.at[1:8], v_s), (osend.at[1:8], o_s), (ssend.at[1:8], st_s), (rest, h_s),
     ):
         remote(sent, sent, sem, part_r, sp, tp).wait_send()
-    pltpu.make_async_copy(rows_out, out, store).wait()
 
 
 def body(
@@ -437,9 +441,9 @@
     dma = pltpu.SemaphoreType.DMA
     return pl.pallas_call(
         kernel,
-        out_shape=jax.ShapeDtypeStruct((ROWS, WIDTH), BF16),
+        out_shape=pltpu.VMEM((ROWS, WIDTH), BF16),
         in_specs=[hbm] * 15,
-        out_specs=hbm,
+        out_specs=pl.BlockSpec(memory_space=pltpu.VMEM),
         scratch_shapes=[
             pltpu.VMEM((1, 256), F32),
             pltpu.VMEM((1, 256), F32),
@@ -447,7 +451,6 @@
             pltpu.VMEM((1, 128), F32),
             pltpu.SMEM((1,), F32),
             pltpu.SMEM((1,), F32),
-            pltpu.VMEM((ROWS, WIDTH), BF16),
             pltpu.VMEM((TP, ROWS, WIDTH), BF16),
             pltpu.VMEM((CTX, WIDTH), BF16),
             pltpu.VMEM((CHUNK, 256), BF16),
@@ -474,12 +477,12 @@
             pltpu.VMEM((RING, 8, BLOCK), F32),
             pltpu.VMEM((TP, ROWS, 128), BF16),
             pltpu.VMEM((TP, ROWS, 128), BF16),
-            dma((15,)), dma(()), dma(()), dma(()), dma(()), dma(()), dma(()), dma((8,)), dma(()), dma((8,)), dma((2,)),
+            dma((15,)), dma(()), dma(()), dma(()), dma(()), dma(()), dma((8,)), dma(()), dma((8,)), dma((2,)),
             dma(()), dma((2, 8)), dma(()), dma((2, 8)), dma(()), dma((2, 8)),
             dma(()), dma((8,)), dma(()), dma((8,)), dma(()), dma(()),
         ],
         compiler_params=pltpu.CompilerParams(
-            collective_id=0, has_side_effects=True, vmem_limit_bytes=60 * 2**20
+            collective_id=0, has_side_effects=True, vmem_limit_bytes=67043328 - 160 * 1024
         ),
         name="whole",
     )(

time: 72.9 us -> 69.8 us (0.957)
  Pallas kernels: 69.8 us -> 67.5 us
  local copies, waits for them, and re-layouts: 1.57 us -> 0.66 us
    pallas_call x1, Pallas kernels: 69.8 us -> 67.5 us  [body(): pl.pallas_call(kernel, out_shape=pltpu.VMEM((ROWS, WIDTH), BF16), in_spec...]
    unnamed x1, local copies, waits for them, and re-layouts: 1.57 us -> 0.66 us
where the time goes in v4:
time: 69.8 us; the launch traced here: 69.4 us
  Pallas kernels  67.5 us (97%)
  between operations  1.31 us (2%)
    pallas_call x1, Pallas kernels, body(): pl.pallas_call(kernel, out_shape=pltpu.VMEM((ROWS, WIDTH), BF16), in_spec...  67.5 us

profile of v4, /device:TPU:1, one launch (start us, length us, event | category | flops | bytes accessed | tf_op | source)
XLA Modules:
  0.0 69.4 jit_solution(16694635327508818304)
XLA Ops:
  1.3 67.5 %whole.1 = bf16[32,2048]{1,0:T(8,128)(2,1)S(1)} custom-call(bf16[32,2048]{1,0:T(8,128)(2,1)} %latent.1, bf16[8,2048]{1,0:T(8,128)(2,1)} %context.1, f32[1,256]{1,0:T(1,128)} %bitcast.13, f32[1,256]{1,0:T(1,128)} %bitcast.14, bf16[96,256]{1,0:T(8,128)(2,1)} %bitcast.12, bf16[64,2048]{1,0:T(8,128)(2,1)} %bitcast.8, bf16[64,2048]{1,0:T(8,128)(2,1)} %bitcast.9, ...), custom_call_target="tpu_custom_call" | custom-call | tf_op jit(solution)/shard_map/whole/pallas_call | solution.py:442
  68.8 0.7 copy.17

commit v5 on v4

--- a/solution.py
+++ b/solution.py
@@ -46,7 +46,7 @@
 def kernel(
     latent, context, cond_in, ccond_in, modw, wq1, wq2, wk1, wk2, wv, lam_in, boost_in, gain_in, wout, freq_in,
     out,
-    cond, ccond, gain, freq, lam, boost,
+    cond, ccond, gain, freq, lam, boost, branch,
     lat, ctx, mw, wqk, wval, wo, part, modg, modv, nlat, nctx, cosb, sinb, qb, kb, vb, vx, kc,
     held, top, osend, ssend, orecv, srecv, hsend, hrecv,
     load, part_s, part_r, z_s, z_r, lat_s, lat_r, wo_s, wo_r, wo2_r,
@@ -328,12 +328,6 @@
     def share(d):
         remote(wo.at[chip(d)], wo.at[chip(d)], wo_s, wo_r.at[chip(d)], sp, partner).start()
 
-    for c, d in ((0, 3), (1, 1)):
-        slot = chip(d)
-        remote(wo.at[slot], wo.at[slot], wo_s, wo_r.at[slot], sp, tp).wait_recv()
-        piece = wo.at[slot, c * 64 : (c + 1) * 64]
-        remote(piece, piece, wo_s, wo2_r.at[c], sp, chip(4 - d)).start()
-    share(3)
     unpack((2, 6))
     for slot in (7, 2, 6):
         work(slot, (0, 1, 7, 2, 6))
@@ -347,6 +341,12 @@
         pass_value(5, 4, c)
         arrived(kb, k_r, 5, c)
         arrived(vb, v_r, 3, c)
+    for c, d in ((0, 3), (1, 1)):
+        slot = chip(d)
+        remote(wo.at[slot], wo.at[slot], wo_s, wo_r.at[slot], sp, tp).wait_recv()
+        piece = wo.at[slot, c * 64 : (c + 1) * 64]
+        remote(piece, piece, wo_s, wo2_r.at[c], sp, chip(4 - d)).start()
+    share(3)
     share(1)
     unpack((3, 5))
     for slot in (5, 3):
@@ -406,24 +406,33 @@
             mixed = mixed + u * weights[:, 8 * n + 4 * m : 8 * n + 4 * m + 1]
     normed = mixed * lax.rsqrt(jnp.mean(mixed * mixed, axis=1, keepdims=True) + EPSILON) * gain[...]
     hsend[...] = normed.astype(BF16).reshape(TP, ROWS, 128)
-    hs = [
-        remote(hsend.at[(tp + d) % TP], hrecv.at[tp], h_s, h_r, sp, (tp + d) % TP)
-        for d in range(1, TP)
-    ]
+    hs = []
+    for d in (2, 1, 3, 0):
+        for n in (core, 1 - core) if d else (1 - core,):
+            to = ((x + d) % 4) * 2 + n
+            hs.append(remote(hsend.at[to], hrecv.at[tp], h_s, h_r.at[1 if d == 2 else 0], sp, to))
     for c in hs:
         c.start()
     hrecv[tp] = hsend[tp]
     for d in range(4):
         slot = ((x + d) % 4) * 2 + 1 - core
         remote(wo.at[slot], wo.at[slot], wo_s, wo_r.at[slot], sp, tp).wait_recv()
-    rest = hrecv.at[0 : TP - 1]
-    remote(rest, rest, h_s, h_r, sp, tp).wait_recv()
-    heads = jnp.concatenate([hrecv[j] for j in range(TP)], axis=1)
+    near_heads, far_heads, rest = hrecv.at[0:5], hrecv.at[0:2], hrecv.at[0 : TP - 1]
+    remote(near_heads, near_heads, h_s, h_r.at[0], sp, tp).wait_recv()
+
+    def branch_of(d, cols):
+        pair = ((x + d) % 4) * 2
+        heads = jnp.concatenate([hrecv[pair], hrecv[pair + 1]], axis=1)
+        return dot(heads, wo[pl.ds(pair, 2), :, cols].reshape(256, 256))
+
     for k in range(WIDTH // 256):
         cols = slice(k * 256, (k + 1) * 256)
-        branch = dot(heads, wo[:, :, cols].reshape(TP * 128, 256))
+        branch[:, cols] = branch_of(0, cols) + branch_of(1, cols) + branch_of(3, cols)
+    remote(far_heads, far_heads, h_s, h_r.at[1], sp, tp).wait_recv()
+    for k in range(WIDTH // 256):
+        cols = slice(k * 256, (k + 1) * 256)
         gate = jnp.concatenate([modv[0, 32 + 2 * k : 33 + 2 * k, :], modv[0, 33 + 2 * k : 34 + 2 * k, :]], axis=1)
-        out[:, cols] = (lat[tp, :, cols].astype(F32) + gate * branch).astype(BF16)
+        out[:, cols] = (lat[tp, :, cols].astype(F32) + gate * (branch[:, cols] + branch_of(2, cols))).astype(BF16)
 
     for sent, sem in (
         (others, part_s), (lat.at[1:8], lat_s), (wo.at[1:8], wo_s), (far_rows, z_s), (qb.at[1:8], q_s), (kb.at[1:8], k_s),
@@ -451,6 +460,7 @@
             pltpu.VMEM((1, 128), F32),
             pltpu.SMEM((1,), F32),
             pltpu.SMEM((1,), F32),
+            pltpu.VMEM((ROWS, WIDTH), F32),
             pltpu.VMEM((TP, ROWS, WIDTH), BF16),
             pltpu.VMEM((CTX, WIDTH), BF16),
             pltpu.VMEM((CHUNK, 256), BF16),
@@ -479,7 +489,7 @@
             pltpu.VMEM((TP, ROWS, 128), BF16),
             dma((15,)), dma(()), dma(()), dma(()), dma(()), dma(()), dma((8,)), dma(()), dma((8,)), dma((2,)),
             dma(()), dma((2, 8)), dma(()), dma((2, 8)), dma(()), dma((2, 8)),
-            dma(()), dma((8,)), dma(()), dma((8,)), dma(()), dma(()),
+            dma(()), dma((8,)), dma(()), dma((8,)), dma(()), dma((2,)),
         ],
         compiler_params=pltpu.CompilerParams(
             collective_id=0, has_side_effects=True, vmem_limit_bytes=67043328 - 160 * 1024

time: 69.8 us -> 69.3 us (level)
  no operation moved by 1% of the time
where the time goes in v5:
time: 69.3 us; the launch traced here: 69.1 us
  Pallas kernels  67.2 us (97%)
  between operations  1.31 us (2%)
    pallas_call x1, Pallas kernels, body(): pl.pallas_call(kernel, out_shape=pltpu.VMEM((ROWS, WIDTH), BF16), in_spec...  67.2 us

profile of v5, /device:TPU:1, one launch (start us, length us, event | category | flops | bytes accessed | tf_op | source)
XLA Modules:
  0.0 69.1 jit_solution(10691293704932097146)
XLA Ops:
  1.3 67.2 %whole.1 = bf16[32,2048]{1,0:T(8,128)(2,1)S(1)} custom-call(bf16[32,2048]{1,0:T(8,128)(2,1)} %latent.1, bf16[8,2048]{1,0:T(8,128)(2,1)} %context.1, f32[1,256]{1,0:T(1,128)} %bitcast.13, f32[1,256]{1,0:T(1,128)} %bitcast.14, bf16[96,256]{1,0:T(8,128)(2,1)} %bitcast.12, bf16[64,2048]{1,0:T(8,128)(2,1)} %bitcast.8, bf16[64,2048]{1,0:T(8,128)(2,1)} %bitcast.9, ...), custom_call_target="tpu_custom_call" | custom-call | tf_op jit(solution)/shard_map/whole/pallas_call | solution.py:451
  68.5 0.7 copy.17
